TPU v7x, 32 devices: a whole 2x2x4 slice. The times are simulated.
32 devices in a mesh: pp: 2 (over x), fs: 4 (over y, core), tp: 4 (over z).
Axes of the slice: x: 2, y: 2, z: 4, core: 2. Of those that a mesh axis runs over, the one named last changes fastest.
Arguments:
- inputs: bfloat16 [512, 2048], P('pp', ('fs', 'tp')), may hold values from -6 to 6
- norm_gain: bfloat16 [2, 2048], P('pp', ('fs', 'tp')), may hold values from 0.099609375 to 1.8984375
- w_value: bfloat16 [2, 2048, 2048], P('pp', None, ('fs', 'tp')), may hold values from -0.125 to 0.125
- w_gate: bfloat16 [2, 2048, 2048], P('pp', None, ('fs', 'tp')), may hold values from -0.125 to 0.125
- w_taps: bfloat16 [2, 31, 2048], P('pp', None, ('fs', 'tp')), may hold values from -1 to 1
- ln_gain: float32 [2, 2048], P('pp', ('fs', 'tp')), may hold values from 0.1 to 1.9
- ln_shift: float32 [2, 2048], P('pp', ('fs', 'tp')), may hold values from -3 to 3
Outputs:
- outputs: bfloat16 [512, 2048], P('pp', ('fs', 'tp'))
All inputs are finite; a program needn't handle non-finite values.
Results may differ from a plain program's by a relative error of at most 0.0085.
Values may be sent and summed in bfloat16 or wider, within the bound.
A program may use at most 64 MiB of HBM per device.

v0:
```python
import functools

import jax
import jax.numpy as jnp
from jax import lax
from jax.experimental import pallas as pl
from jax.experimental.pallas import tpu as pltpu
from jax.sharding import PartitionSpec as P

LEN = 128


norm_eps = 1e-06
layer_eps = 1e-05
MESH = pl.DeviceIdType.MESH


def kernel(
    sizes,
    x_hbm,
    gain_hbm,
    wv_hbm,
    wg_hbm,
    taps_hbm,
    lgain_hbm,
    lshift_hbm,
    out_ref,
    x_ref,
    gain_ref,
    wv_ref,
    wg_ref,
    taps_ref,
    lgain_ref,
    lshift_ref,
    load_sem,
    gath,
    gains,
    stat,
    hbuf,
    pad,
    taps,
    conv_buf,
    new_buf,
    turn,
    gath_sem,
    gain_sem,
    stat_sem,
    out_sem,
    feed_send,
    relay_send,
    gain_send,
    stat_send,
    next_send,
    back_send,
):
    P_, F, T = sizes
    G = F * T
    k, f, t = lax.axis_index("pp"), lax.axis_index("fs"), lax.axis_index("tp")
    M = gath.shape[0]
    C = x_ref.shape[1]
    D = wv_ref.shape[1]
    own_rows = x_ref.shape[0]
    piece = min(LEN, own_rows)
    per_mb = LEN // piece
    per_owner = own_rows // piece
    head = pad.shape[0] - LEN
    me = f * T + t
    loads = [
        pltpu.make_async_copy(a, b, load_sem.at[n])
        for n, (a, b) in enumerate(
            [
                (x_hbm, x_ref), (gain_hbm, gain_ref), (wv_hbm, wv_ref), (wg_hbm, wg_ref),
                (taps_hbm, taps_ref), (lgain_hbm, lgain_ref), (lshift_hbm, lshift_ref),
            ]
        )
    ]
    for load in loads:
        load.start()
    if T & (T - 1) == 0:
        to_t = [t] + [t ^ d for d in range(T - 1, 0, -1)]
        from_t = to_t
    else:
        to_t = [lax.rem(t + d, T) for d in range(T)]
        from_t = [lax.rem(t + T - d, T) for d in range(T)]

    def at(kk, ff, tt):
        return {"pp": kk, "fs": ff, "tp": tt}

    def send(src, dst, s_sem, r_sem, dev, cond=None):
        def go():
            pltpu.make_async_remote_copy(
                src_ref=src, dst_ref=dst, send_sem=s_sem, recv_sem=r_sem,
                device_id=dev, device_id_type=MESH,
            ).start()

        if cond is None:
            go()
        else:
            pl.when(cond)(go)

    def await_bytes(ref, sem):
        pltpu.make_async_copy(ref, ref, sem).wait()

    peers = []
    for dt in list(range(1, T)) + [0]:
        for df in range(F):
            if df or dt:
                peers.append(at(k, lax.rem(f + df, F), to_t[dt]))
    others = []
    for dk in range(1, P_):
        for dt in range(T):
            others.append(at(lax.rem(k + dk, P_), f, to_t[dt]))
    barrier = pltpu.get_barrier_semaphore()
    for dev in peers + others:
        pl.semaphore_signal(barrier, inc=1, device_id=dev, device_id_type=MESH)
    for load in loads[:2]:
        load.wait()
    gains[me] = gain_ref[...].astype(jnp.float32)
    pad[0:head, :] = jnp.zeros((head, C), jnp.float32)
    turn[...] = jnp.zeros_like(turn)
    pl.semaphore_wait(barrier, len(peers) + len(others))

    for i in range(per_owner):
        p = k * per_owner + i
        m = lax.div(p, per_mb)
        rows = pl.ds(pl.multiple_of(lax.rem(p, per_mb) * piece, piece), piece)
        src = x_ref.at[pl.ds(i * piece, piece)]
        dst = gath.at[m, me, rows]
        sem = gath_sem.at[m, me]

        @pl.when(k == 0)
        def _():
            pltpu.make_async_copy(src, dst, sem).start()

        send(src, dst, feed_send.at[0], sem, at(0, f, t), k != 0)
        for dt in range(1, T):
            send(src, dst, feed_send.at[1], sem, at(0, f, to_t[dt]))
        if i == 0:
            for dev in peers:
                send(gains.at[me], gains.at[me], gain_send.at[0], gain_sem.at[0], dev)
    for load in loads[2:]:
        load.wait()
    taps[...] = taps_ref[0].astype(jnp.float32)

    bits = []
    b = F // 2
    while b:
        bits.append(b)
        b //= 2

    def relay(m, low):
        for r in range(F):
            if ((r & -r) if r else F) == low:
                for tt in from_t:
                    slot = (f ^ r) * T + tt
                    block = gath.at[m, slot]
                    await_bytes(block, gath_sem.at[m, slot])
                    for b in bits:
                        if b < low:
                            send(block, block, relay_send.at[0], gath_sem.at[m, slot], at(k, f ^ b, t))

    def project(m):
        squares = jnp.zeros((LEN, C), jnp.float32)
        for s in range(G):
            xf = gath[m, s].astype(jnp.float32)
            squares = squares + xf * xf
            hbuf[:, s * C : (s + 1) * C] = (xf * gains[s]).astype(jnp.bfloat16)
        scale = lax.rsqrt(jnp.sum(squares, axis=1, keepdims=True) / D + norm_eps)
        value = jnp.dot(hbuf[...], wv_ref[0], preferred_element_type=jnp.float32) * scale
        gate = jnp.dot(hbuf[...], wg_ref[0], preferred_element_type=jnp.float32) * scale
        pad[head:, :] = value * jax.nn.sigmoid(gate)
        W = taps.shape[0]
        step = 32
        for r0 in range(0, LEN, step):
            acc = jnp.zeros((step, C), jnp.float32)
            for j in range(W):
                o = head - (W - 1) + j + r0
                acc = acc + pad[o : o + step, :] * taps[j : j + 1, :]
            conv_buf[m, r0 : r0 + step, :] = acc
        conv = conv_buf[m]
        lane = lax.broadcasted_iota(jnp.int32, (LEN, LEN), 1)
        s1 = jnp.sum(conv, axis=1, keepdims=True)
        s2 = jnp.sum(conv * conv, axis=1, keepdims=True)
        both = jnp.where(lane == 0, s1, jnp.where(lane == 1, s2, 0.0))
        stat[m, me] = both.T[0:2, :]
        for dev in peers:
            send(stat.at[m, me], stat.at[m, me], stat_send.at[0], stat_sem.at[m], dev)

    def finish(m):
        await_bytes(stat.at[m, pl.ds(0, G - 1)], stat_sem.at[m])
        turn[0:2, :] = jnp.sum(stat[m], axis=0)
        cols = turn[...].T
        mu = cols[:, 0:1] / D
        var = cols[:, 1:2] / D - mu * mu
        y = (conv_buf[m] - mu) * lax.rsqrt(var + layer_eps) * lgain_ref[...] + lshift_ref[...]
        new = (gath[m, me].astype(jnp.float32) + y * jax.nn.sigmoid(y)).astype(jnp.bfloat16)
        new_buf[m] = new
        if P_ > 1:
            for tt in to_t:
                send(
                    new_buf.at[m], gath.at[m, me], next_send.at[0], gath_sem.at[m, me],
                    at(lax.rem(k + 1, P_), f, tt), k < P_ - 1,
                )
        for q in range(per_mb):
            p = m * per_mb + q
            owner, i = p // per_owner, p % per_owner
            rows = pl.ds(i * piece, piece)
            part = pl.ds(q * piece, piece)
            if owner == P_ - 1:
                @pl.when(k == P_ - 1)
                def _():
                    out_ref[rows, :] = new_buf[m, part, :]
            else:
                send(
                    new_buf.at[m, part], out_ref.at[rows], back_send.at[0], out_sem.at[i],
                    at(owner, f, t), k == P_ - 1,
                )

    levels = [F] + bits

    def run(ahead, lag):
        for m in range(min(ahead, M)):
            relay(m, F)
        for m in range(M):
            if ahead == 1 and m + 1 < M:
                relay(m + 1, F)
            for low in levels[1:-1]:
                relay(m, low)
            if ahead > 1 and m + ahead < M:
                relay(m + ahead, F)
            if lag > 1 and m > 1:
                finish(m - 2)
            if len(levels) > 1:
                relay(m, levels[-1])
            if m == 0:
                await_bytes(gains.at[pl.ds(0, G - 1)], gain_sem.at[0])
            project(m)
            if lag == 1 and m:
                finish(m - 1)
        if lag > 1 and M > 1:
            finish(M - 2)

    if P_ == 1:
        run(2, 1)
    else:
        pl.when(k == 0)(lambda: run(1, 1))
        pl.when(k != 0)(lambda: run(1, 2))
    await_bytes(gath.at[:, pl.ds(0, T * (F - 1))], relay_send.at[0])
    await_bytes(stat.at[:, pl.ds(0, G - 1)], stat_send.at[0])
    await_bytes(gains.at[pl.ds(0, G - 1)], gain_send.at[0])
    for i in range(per_owner):
        await_bytes(gath.at[0, pl.ds(0, T - 1), pl.ds(0, piece)], feed_send.at[1])
    if P_ > 1:
        @pl.when(k != 0)
        def _():
            await_bytes(x_ref, feed_send.at[0])

    finish(M - 1)
    if P_ > 1:
        @pl.when(k < P_ - 1)
        def _():
            await_bytes(gath.at[:, pl.ds(0, T)], next_send.at[0])
            for i in range(per_owner):
                await_bytes(out_ref.at[pl.ds(i * piece, piece)], out_sem.at[i])

        @pl.when(k == P_ - 1)
        def _():
            for _i in range(per_owner * (P_ - 1)):
                await_bytes(out_ref.at[pl.ds(0, piece)], back_send.at[0])


def local(sizes, inputs, norm_gain, w_value, w_gate, w_taps, ln_gain, ln_shift):
    P_, F, T = sizes
    G = F * T
    own_rows, C = inputs.shape
    M = own_rows * P_ // LEN
    piece = min(LEN, own_rows)
    per_owner = own_rows // piece
    per_mb = LEN // piece
    D = w_value.shape[1]
    W = w_taps.shape[1]
    head = -(-(W - 1) // 8) * 8
    operands = (inputs, norm_gain, w_value, w_gate, w_taps, ln_gain, ln_shift)
    dma = pltpu.SemaphoreType.DMA
    f32, bf16 = jnp.float32, jnp.bfloat16
    return pl.pallas_call(
        functools.partial(kernel, sizes),
        out_shape=jax.ShapeDtypeStruct((own_rows, C), bf16),
        in_specs=[pl.BlockSpec(memory_space=pl.ANY)] * 7,
        out_specs=pl.BlockSpec(memory_space=pltpu.VMEM),
        scratch_shapes=[
            *[pltpu.VMEM(a.shape, a.dtype) for a in operands],
            dma((len(operands),)),
            pltpu.VMEM((M, G, LEN, C), bf16),
            pltpu.VMEM((G, 1, C), f32),
            pltpu.VMEM((M, G, 2, LEN), f32),
            pltpu.VMEM((LEN, D), bf16),
            pltpu.VMEM((LEN + head, C), f32),
            pltpu.VMEM((W, C), f32),
            pltpu.VMEM((M, LEN, C), f32),
            pltpu.VMEM((M, LEN, C), bf16),
            pltpu.VMEM((LEN, LEN), f32),
            dma((M, G)),
            dma((1,)),
            dma((M,)),
            dma((per_owner,)),
            dma((2,)),
            dma((1,)),
            dma((1,)),
            dma((1,)),
            dma((1,)),
            dma((1,)),
        ],
        compiler_params=pltpu.CompilerParams(collective_id=0, has_side_effects=True),
    )(*operands)


def solution(mesh):
    sizes = (mesh.shape["pp"], mesh.shape["fs"], mesh.shape["tp"])
    in_specs = (
        P("pp", ("fs", "tp")),
        P("pp", ("fs", "tp")),
        P("pp", None, ("fs", "tp")),
        P("pp", None, ("fs", "tp")),
        P("pp", None, ("fs", "tp")),
        P("pp", ("fs", "tp")),
        P("pp", ("fs", "tp")),
    )
    out_specs = P("pp", ("fs", "tp"))
    return jax.shard_map(
        functools.partial(local, sizes), mesh=mesh, in_specs=in_specs, out_specs=out_specs,
        check_vma=False,
    )
```

profile of v0, /device:TPU:3, one launch (start us, length us, event | category | flops | bytes accessed | tf_op | source)
XLA Modules:
  0.0 48.3 jit_solution(18305948279456401567)
XLA Ops:
  0.0 46.8 %shard_map.73 = bf16[256,128]{1,0:T(8,128)(2,1)} custom-call(bf16[256,128]{1,0:T(8,128)(2,1)} %x_hbm.1, bf16[1,128]{1,0:T(2,128)(2,1)} %gain_hbm.1, bf16[1,2048,128]{2,1,0:T(8,128)(2,1)} %wv_hbm.1, bf16[1,2048,128]{2,1,0:T(8,128)(2,1)} %wg_hbm.1, bf16[1,31,128]{2,1,0:T(8,128)(2,1)} %taps_hbm.1, f32[1,128]{1,0:T(1,128)} %lgain_hbm.1, f32[1,128]{1,0:T(1,128)} %lshift_hbm.1), custom_call_target="tpu_custom_call" | custom-call | tf_op jit(solution)/shard_map/pallas_call | solution.py:286
  46.8 1.5 %copy.9 = bf16[256,128]{1,0:T(8,128)(2,1)} copy(bf16[256,128]{1,0:T(8,128)(2,1)} %shard_map.73) | data formatting | bytes 131072
where the time goes:
time: 48.5 us; the launch traced here: 48.3 us
  Pallas kernels  46.8 us (96%)
  local copies, waits for them, and re-layouts  1.47 us (3%)
    pallas_call x1, Pallas kernels, local(): pl.pallas_call(functools.partial(kernel, sizes), out_shape=jax.ShapeDtype...  46.8 us
    unnamed x1, local copies, waits for them, and re-layouts  1.47 us

commit v1 on v0

v1 whole, which is shorter than its diff:
```python
import functools

import jax
import jax.numpy as jnp
from jax import lax
from jax.experimental import pallas as pl
from jax.experimental.pallas import tpu as pltpu
from jax.sharding import PartitionSpec as P

LEN = 128
CHUNK = 64
LAGS = (0, 1, 2)
AHEAD = 4

norm_eps = 1e-06
layer_eps = 1e-05
MESH = pl.DeviceIdType.MESH


def kernel(
    sizes,
    x_hbm,
    gain_hbm,
    wv_hbm,
    wg_hbm,
    taps_hbm,
    lgain_hbm,
    lshift_hbm,
    out_ref,
    x_ref,
    gain_ref,
    wcat,
    taps_ref,
    lgain_ref,
    lshift_ref,
    load_sem,
    sg,
    cg,
    hb,
    gains,
    lng,
    lnb,
    sin,
    sfin,
    sout,
    pad,
    taps,
    conv_own,
    conv_out,
    s_own,
    new_buf,
    turn,
    s_sem,
    c_sem,
    sin_sem,
    sfin_sem,
    gain_sem,
    out_sem,
    feed_send,
    relay_send,
    small_send,
    stat_send,
    next_send,
    back_send,
):
    P_, F, T = sizes
    G = F * T
    k, f, t = lax.axis_index("pp"), lax.axis_index("fs"), lax.axis_index("tp")
    NC, R, C = conv_own.shape
    D = wcat.shape[0]
    W = taps.shape[0]
    own_rows = x_ref.shape[0]
    per_owner = own_rows // R
    per_seq = LEN // R
    head = pad.shape[0] - LEN
    me = f * T + t
    feeds = min(2, P_)

    loads = [
        pltpu.make_async_copy(a, b, load_sem.at[n])
        for n, (a, b) in enumerate(
            [
                (x_hbm, x_ref), (gain_hbm, gain_ref), (lgain_hbm, lgain_ref), (lshift_hbm, lshift_ref),
                (taps_hbm, taps_ref),
                (wv_hbm.at[0], wcat.at[:, pl.ds(0, C)]), (wg_hbm.at[0], wcat.at[:, pl.ds(C, C)]),
            ]
        )
    ]
    for load in loads:
        load.start()

    def own_copies():
        for i in range(per_owner):
            n = k * per_owner + i
            pltpu.make_async_copy(x_hbm.at[pl.ds(i * R, R)], sg.at[n, me], s_sem.at[n, me]).start()

    if P_ > 2:
        pl.when(k < feeds)(own_copies)
    else:
        own_copies()

    if T & (T - 1) == 0:
        to_t = [t] + [t ^ d for d in range(1, T)]
        from_t = to_t
    else:
        to_t = [lax.rem(t + d, T) for d in range(T)]
        from_t = [lax.rem(t + T - d, T) for d in range(T)]

    def at(kk, ff, tt):
        return {"pp": kk, "fs": ff, "tp": tt}

    def send(src, dst, s_sem_, r_sem, dev):
        pltpu.make_async_remote_copy(
            src_ref=src, dst_ref=dst, send_sem=s_sem_, recv_sem=r_sem, device_id=dev, device_id_type=MESH
        ).start()

    def await_bytes(ref, sem):
        pltpu.make_async_copy(ref, ref, sem).wait()

    peers = [at(k, lax.rem(f + df, F), to_t[dt]) for dt in range(T - 1, -1, -1) for df in range(F) if df or dt]

    def plane(kk):
        return [at(kk, lax.rem(f + df, F), to_t[dt]) for dt in range(T - 1, -1, -1) for df in range(F)]

    barrier = pltpu.get_barrier_semaphore()
    everyone = peers + [dev for dk in range(1, P_) for dev in plane(lax.rem(k + dk, P_))]
    for dev in everyone:
        pl.semaphore_signal(barrier, inc=1, device_id=dev, device_id_type=MESH)
    for load in loads[:4]:
        load.wait()
    gains[me] = gain_ref[...].astype(jnp.float32)
    lgain_ref[...] = lgain_ref[...] * 0.5
    lshift_ref[...] = lshift_ref[...] * 0.5
    pad[0:head, :] = jnp.zeros((head, C), jnp.float32)
    turn[...] = jnp.zeros_like(turn)
    pl.semaphore_wait(barrier, len(everyone))

    for q in range(feeds):
        for i in range(per_owner):
            n = k * per_owner + i
            src = x_ref.at[pl.ds(i * R, R)]
            for dt in range(T - 1, 0, -1):
                send(src, sg.at[n, me], feed_send.at[0], s_sem.at[n, me], at(q, f, to_t[dt]))
            if P_ > 1:
                @pl.when(k != q)
                def _():
                    send(src, sg.at[n, me], feed_send.at[0], s_sem.at[n, me], at(q, f, t))
            if q == 0 and i == 0:
                for dev in peers:
                    send(gains.at[me], gains.at[me], small_send.at[0], gain_sem.at[0], dev)

    bits = []
    b = F // 2
    while b:
        bits.append(b)
        b //= 2
    levels = [F] + bits

    def hop(buf, sem, n, low):
        for r in range(F):
            if ((r & -r) if r else F) == low:
                for tt in from_t:
                    slot = (f ^ r) * T + tt
                    block = buf.at[n, slot]
                    await_bytes(block, sem.at[n, slot])
                    for b in bits:
                        if b < low:
                            send(block, block, relay_send.at[0], sem.at[n, slot], at(k, f ^ b, t))

    def prepare():
        for load in loads[4:]:
            load.wait()
        taps[...] = taps_ref[0].astype(jnp.float32)
        await_bytes(gains.at[pl.ds(0, G - 1)], gain_sem.at[0])
        for s in range(G):
            turn[s : s + 1, :] = gains[s]
        cols = turn[...].T
        for s in range(G):
            rows = pl.ds(s * C, C)
            wcat[rows, :] = (wcat[rows, :].astype(jnp.float32) * cols[:, s : s + 1]).astype(jnp.bfloat16)

    def moments(ref, n):
        turn[0:2, :] = jnp.sum(ref[n], axis=0)
        cols = turn[...].T
        mu = cols[0:R, 0:1] / D
        var = cols[0:R, 1:2] / D - mu * mu
        return mu, lax.rsqrt(var + layer_eps)

    def enter(n):
        mu, rs = moments(sin, n)
        blocks = []
        for s in range(G):
            half = (cg[n, s].astype(jnp.float32) - mu) * rs * lng[s] + lnb[s]
            new = (sg[n, s].astype(jnp.float32) + (half + half * jnp.tanh(half))).astype(jnp.bfloat16)
            hb[s] = new
            blocks.append(new)
        s_own[n] = hb[me]
        return blocks

    def project(n, blocks):
        squares = jnp.zeros((R, C), jnp.float32)
        for xb in blocks:
            xf = xb.astype(jnp.float32)
            squares = squares + xf * xf
        scale = lax.rsqrt(jnp.sum(squares, axis=1, keepdims=True) / D + norm_eps)
        both = jnp.dot(jnp.concatenate(blocks, axis=1), wcat[...], preferred_element_type=jnp.float32) * scale
        j = (n % per_seq) * R
        pad[head + j : head + j + R, :] = both[:, :C] * (0.5 + 0.5 * jnp.tanh(0.5 * both[:, C:]))
        step = 32
        for r0 in range(0, R, step):
            acc = jnp.zeros((step, C), jnp.float32)
            for w in range(W):
                o = head - (W - 1) + w + j + r0
                acc = acc + pad[o : o + step, :] * taps[w : w + 1, :]
            conv_own[n, r0 : r0 + step, :] = acc
        conv = conv_own[n]
        lane = lax.broadcasted_iota(jnp.int32, (R, LEN), 1)
        s1 = jnp.sum(conv, axis=1, keepdims=True)
        s2 = jnp.sum(conv * conv, axis=1, keepdims=True)
        turn[0:R, :] = jnp.where(lane == 0, s1, jnp.where(lane == 1, s2, 0.0))
        return conv, turn[...].T[0:2, :]

    def pass_on(n, first):
        conv, stat = project(n, [sg[n, s] for s in range(G)] if first else enter(n))
        sout[n] = stat
        conv_out[n] = conv.astype(jnp.bfloat16)
        if not first:
            for tt in to_t[::-1]:
                send(s_own.at[n], sg.at[n, me], next_send.at[0], s_sem.at[n, me], at(k + 1, f, tt))
        for dev in plane(k + 1):
            send(sout.at[n], sin.at[n, me], stat_send.at[0], sin_sem.at[n], dev)
        for tt in to_t[::-1]:
            send(conv_out.at[n], cg.at[n, me], next_send.at[0], c_sem.at[n, me], at(k + 1, f, tt))

    def last_stats(n, first):
        _, stat = project(n, [sg[n, s] for s in range(G)] if first else enter(n))
        sfin[n, me] = stat
        for dev in peers:
            send(sfin.at[n, me], sfin.at[n, me], stat_send.at[0], sfin_sem.at[n], dev)

    def finish(n, first):
        await_bytes(sfin.at[n, pl.ds(0, G - 1)], sfin_sem.at[n])
        mu, rs = moments(sfin, n)
        half = (conv_own[n] - mu) * rs * lgain_ref[...] + lshift_ref[...]
        stream = sg[n, me] if first else s_own[n]
        new = (stream.astype(jnp.float32) + (half + half * jnp.tanh(half))).astype(jnp.bfloat16)
        owner, i = n // per_owner, n % per_owner
        rows = pl.ds(i * R, R)
        if owner == P_ - 1:
            out_ref[rows, :] = new
        else:
            new_buf[n] = new
            send(new_buf.at[n], out_ref.at[rows], back_send.at[0], out_sem.at[i], at(owner, f, t))

    def staged(buf, sem, i, upto=None):
        for low, lag in list(zip(levels, LAGS))[:upto]:
            if 0 <= i - lag < NC:
                hop(buf, sem, i - lag, low)

    depth = LAGS[len(levels) - 1]

    def run(first, last):
        step = last_stats if last else pass_on
        if first:
            if not last:
                for dev in plane(k + 1):
                    send(lgain_ref, lng.at[me], small_send.at[1], gain_sem.at[1], dev)
                    send(lshift_ref, lnb.at[me], small_send.at[1], gain_sem.at[2], dev)
            for i in range(NC + depth):
                staged(sg, s_sem, i)
                n = i - depth
                if n == 0:
                    prepare()
                if n >= 0:
                    step(n, True)
                    if last and n >= 2:
                        finish(n - 2, True)
        else:
            if not last:
                for dev in plane(k + 1):
                    send(lgain_ref, lng.at[me], small_send.at[1], gain_sem.at[1], dev)
                    send(lshift_ref, lnb.at[me], small_send.at[1], gain_sem.at[2], dev)
            for i in range(min(AHEAD, NC) + depth):
                staged(sg, s_sem, i)
            prepare()
            await_bytes(lng.at[pl.ds(0, G)], gain_sem.at[1])
            await_bytes(lnb.at[pl.ds(0, G)], gain_sem.at[2])
            for i in range(NC + depth):
                staged(cg, c_sem, i)
                n = i - depth
                if i + min(AHEAD, NC) + depth < NC + depth:
                    staged(sg, s_sem, i + min(AHEAD, NC) + depth)
                if n >= 0:
                    await_bytes(sin.at[n, pl.ds(0, G)], sin_sem.at[n])
                    step(n, False)
                    if last and n >= 2:
                        finish(n - 2, False)
        if last:
            for n in range(max(NC - 2, 0), NC):
                finish(n, first)
        hops = T * (F - 1)
        if hops:
            await_bytes(sg.at[:, pl.ds(0, hops)], relay_send.at[0])
            if not first:
                await_bytes(cg.at[:, pl.ds(0, hops)], relay_send.at[0])
        await_bytes(gains.at[pl.ds(0, G - 1)], small_send.at[0])
        if last:
            await_bytes(sfin.at[:, pl.ds(0, G - 1)], stat_send.at[0])
            for _ in range(per_owner * (P_ - 1)):
                await_bytes(out_ref.at[pl.ds(0, R)], back_send.at[0])
        else:
            await_bytes(sin.at[:, pl.ds(0, G)], stat_send.at[0])
            await_bytes(lng.at[pl.ds(0, G)], small_send.at[1])
            await_bytes(lnb.at[pl.ds(0, G)], small_send.at[1])
            await_bytes(cg.at[:, pl.ds(0, T)], next_send.at[0])
            if not first:
                await_bytes(sg.at[:, pl.ds(0, T)], next_send.at[0])

    if P_ == 1:
        run(True, True)
    else:
        pl.when(k == 0)(lambda: run(True, False))
        pl.when(k == P_ - 1)(lambda: run(False, True))
        if P_ > 2:
            pl.when((k > 0) & (k < P_ - 1))(lambda: run(False, False))

    for _ in range(per_owner):
        await_bytes(sg.at[0, pl.ds(0, feeds * T - 1)], feed_send.at[0])
    if P_ > 2:
        @pl.when(k >= feeds)
        def _():
            await_bytes(x_ref, feed_send.at[0])
    if P_ > 1:
        @pl.when(k < P_ - 1)
        def _():
            for i in range(per_owner):
                await_bytes(out_ref.at[pl.ds(i * R, R)], out_sem.at[i])


def local(sizes, inputs, norm_gain, w_value, w_gate, w_taps, ln_gain, ln_shift):
    P_, F, T = sizes
    G = F * T
    own_rows, C = inputs.shape
    R = min(CHUNK, own_rows)
    NC = own_rows * P_ // R
    D = w_value.shape[1]
    W = w_taps.shape[1]
    head = -(-(W - 1) // 8) * 8
    operands = (inputs, norm_gain, w_value, w_gate, w_taps, ln_gain, ln_shift)
    dma = pltpu.SemaphoreType.DMA
    f32, bf16 = jnp.float32, jnp.bfloat16
    V = pltpu.VMEM
    return pl.pallas_call(
        functools.partial(kernel, sizes),
        out_shape=jax.ShapeDtypeStruct((own_rows, C), bf16),
        in_specs=[pl.BlockSpec(memory_space=pl.ANY)] * 7,
        out_specs=pl.BlockSpec(memory_space=pltpu.VMEM),
        scratch_shapes=[
            V(inputs.shape, bf16), V(norm_gain.shape, bf16), V((D, 2 * C), bf16), V(w_taps.shape, bf16),
            V(ln_gain.shape, f32), V(ln_shift.shape, f32),
            dma((len(operands),)),
            V((NC, G, R, C), bf16), V((NC, G, R, C), bf16), V((G, R, C), bf16),
            V((G, 1, C), f32), V((G, 1, C), f32), V((G, 1, C), f32),
            V((NC, G, 2, LEN), f32), V((NC, G, 2, LEN), f32), V((NC, 2, LEN), f32),
            V((LEN + head, C), f32), V((W, C), f32),
            V((NC, R, C), f32), V((NC, R, C), bf16), V((NC, R, C), bf16), V((NC, R, C), bf16),
            V((LEN, LEN), f32),
            dma((NC, G)), dma((NC, G)), dma((NC,)), dma((NC,)), dma((3,)), dma((own_rows // R,)),
            dma((1,)), dma((1,)), dma((2,)), dma((1,)), dma((1,)), dma((1,)),
        ],
        compiler_params=pltpu.CompilerParams(collective_id=0, has_side_effects=True),
    )(*operands)


def solution(mesh):
    sizes = (mesh.shape["pp"], mesh.shape["fs"], mesh.shape["tp"])
    in_specs = (
        P("pp", ("fs", "tp")),
        P("pp", ("fs", "tp")),
        P("pp", None, ("fs", "tp")),
        P("pp", None, ("fs", "tp")),
        P("pp", None, ("fs", "tp")),
        P("pp", ("fs", "tp")),
        P("pp", ("fs", "tp")),
    )
    out_specs = P("pp", ("fs", "tp"))
    return jax.shard_map(
        functools.partial(local, sizes), mesh=mesh, in_specs=in_specs, out_specs=out_specs,
        check_vma=False,
    )
```

time: 48.5 us -> 62.2 us (1.28)
  Pallas kernels: 46.8 us -> 60.5 us
    pallas_call x1, Pallas kernels: 46.8 us -> 60.5 us  [local(): pl.pallas_call(functools.partial(kernel, sizes), out_shape=jax.ShapeDtype...]
where the time goes in v1:
time: 62.2 us; the launch traced here: 62 us
  Pallas kernels  60.5 us (97%)
  local copies, waits for them, and re-layouts  1.47 us (2%)
    pallas_call x1, Pallas kernels, local(): pl.pallas_call(functools.partial(kernel, sizes), out_shape=jax.ShapeDtype...  60.5 us
    unnamed x1, local copies, waits for them, and re-layouts  1.47 us

profile of v1, /device:TPU:3, one launch (start us, length us, event | category | flops | bytes accessed | tf_op | source)
XLA Modules:
  0.0 62.0 jit_solution(11447150555929546576)
XLA Ops:
  0.0 60.5 %shard_map.73 = bf16[256,128]{1,0:T(8,128)(2,1)} custom-call(bf16[256,128]{1,0:T(8,128)(2,1)} %x_hbm.1, bf16[1,128]{1,0:T(2,128)(2,1)} %gain_hbm.1, bf16[1,2048,128]{2,1,0:T(8,128)(2,1)} %wv_hbm.1, bf16[1,2048,128]{2,1,0:T(8,128)(2,1)} %wg_hbm.1, bf16[1,31,128]{2,1,0:T(8,128)(2,1)} %taps_hbm.1, f32[1,128]{1,0:T(1,128)} %lgain_hbm.1, f32[1,128]{1,0:T(1,128)} %lshift_hbm.1), custom_call_target="tpu_custom_call" | custom-call | tf_op jit(solution)/shard_map/pallas_call | solution.py:353
  60.5 1.5 %copy.9 = bf16[256,128]{1,0:T(8,128)(2,1)} copy(bf16[256,128]{1,0:T(8,128)(2,1)} %shard_map.73) | data formatting | bytes 131072

commit v2 on v1

v2 whole, which is shorter than its diff:
```python
import functools

import jax
import jax.numpy as jnp
from jax import lax
from jax.experimental import pallas as pl
from jax.experimental.pallas import tpu as pltpu
from jax.sharding import PartitionSpec as P

LEN = 128
SPLITS = ((128, 128), (128, 128))
FEED = (2, 3, 1)
SEND = (3, 2, 1, 0)
ENTER = (0, 1, 3, 2)
XCARRY = (1, 2)
ZRELAY = (1, 2)
SWAP = 256
TIMES = ()


norm_eps = 1e-06
layer_eps = 1e-05
MESH = pl.DeviceIdType.MESH


def kernel(
    sizes,
    x_hbm,
    gain_hbm,
    wv_hbm,
    wg_hbm,
    taps_hbm,
    lgain_hbm,
    lshift_hbm,
    out_ref,
    x_ref,
    gain_ref,
    wcat,
    taps_ref,
    lgain_ref,
    lshift_ref,
    load_sem,
    sg,
    cg,
    hg,
    gains,
    lng,
    lnb,
    sin,
    sfin,
    sout,
    pad,
    taps,
    conv_own,
    conv_out,
    keep,
    new_buf,
    turn,
    s_sem,
    c_sem,
    h_sem,
    sin_sem,
    sfin_sem,
    gain_sem,
    out_sem,
    feed_send,
    relay_send,
    small_send,
    stat_send,
    next_send,
    back_send,
    side,
    side_sem,
    swap_send,
):
    P_, F, T = sizes
    G = F * T
    k, f, t = lax.axis_index("pp"), lax.axis_index("fs"), lax.axis_index("tp")
    C = conv_own.shape[1]
    D = wcat.shape[0]
    W = taps.shape[0]
    own_rows = x_ref.shape[0]
    head = pad.shape[0] - LEN
    me = f * T + t
    feeds = min(2, P_)

    loads = [
        pltpu.make_async_copy(a, b, load_sem.at[n])
        for n, (a, b) in enumerate(
            [
                (x_hbm, x_ref), (gain_hbm, gain_ref), (lgain_hbm, lgain_ref), (lshift_hbm, lshift_ref),
                (taps_hbm, taps_ref),
                (wv_hbm.at[0], wcat.at[:, pl.ds(0, C)]), (wg_hbm.at[0], wcat.at[:, pl.ds(C, C)]),
            ]
        )
    ]
    for load in loads:
        load.start()

    if T & (T - 1) == 0:
        to_t = [t] + [t ^ d for d in range(1, T)]
        from_t = to_t
    else:
        to_t = [lax.rem(t + d, T) for d in range(T)]
        from_t = [lax.rem(t + T - d, T) for d in range(T)]

    def at(kk, ff, tt):
        return {"pp": kk, "fs": ff, "tp": tt}

    def send(src, dst, s_sem_, r_sem, dev):
        pltpu.make_async_remote_copy(
            src_ref=src, dst_ref=dst, send_sem=s_sem_, recv_sem=r_sem, device_id=dev, device_id_type=MESH
        ).start()

    def await_bytes(ref, sem):
        pltpu.make_async_copy(ref, ref, sem).wait()

    peers = [at(k, lax.rem(f + df, F), to_t[dt]) for dt in range(T - 1, -1, -1) for df in range(F) if df or dt]

    def plane(kk):
        return [at(kk, lax.rem(f + df, F), to_t[dt]) for dt in range(T - 1, -1, -1) for df in range(F)]

    pow2 = T & (T - 1) == 0
    every = tuple(range(T))
    chunks, cross = plan(sizes, own_rows)
    NCH = len(chunks)
    zrelay = ZRELAY if pow2 and T == 4 else ()

    def rows_of(n):
        return pl.ds(chunks[n][0], chunks[n][1])

    def feed(q, dts, mine):
        for n, start, i in mine:
            size = chunks[n][1] if cross else chunks[0][1]
            for dt in dts:
                send(
                    x_ref.at[pl.ds(i, size)], sg.at[me, pl.ds(start, size)], feed_send.at[0], s_sem.at[n, me],
                    at(q, f, to_t[dt]),
                )

    def own_copies(mine):
        for n, start, i in mine:
            size = chunks[n][1] if cross else chunks[0][1]
            pltpu.make_async_copy(
                x_hbm.at[pl.ds(i, size)], sg.at[me, pl.ds(start, size)], s_sem.at[n, me]
            ).start()

    def mine_of(kk):
        return [(n, c, c % own_rows) for n, (c, _) in enumerate(chunks) if c // own_rows == kk]

    if cross:
        for kk in range(P_):
            pl.when(k == kk)(functools.partial(own_copies, mine_of(kk)))
    else:
        size = chunks[0][1]
        mine = [(k * (own_rows // size) + i, k * own_rows + i * size, i * size) for i in range(own_rows // size)]
        if P_ > feeds:
            pl.when(k < feeds)(functools.partial(own_copies, mine))
        else:
            own_copies(mine)
    barrier = pltpu.get_barrier_semaphore()
    everyone = peers + [dev for dk in range(1, P_) for dev in plane(lax.rem(k + dk, P_))]
    for dev in everyone:
        pl.semaphore_signal(barrier, inc=1, device_id=dev, device_id_type=MESH)
    for load in loads[:4]:
        load.wait()
    gains[me] = gain_ref[...].astype(jnp.float32)
    lgain_ref[...] = lgain_ref[...] * 0.5
    lshift_ref[...] = lshift_ref[...] * 0.5
    pad[0:head, :] = jnp.zeros((head, C), jnp.float32)
    turn[...] = jnp.zeros_like(turn)
    pl.semaphore_wait(barrier, len(everyone))

    def greet():
        for dev in peers:
            send(gains.at[me], gains.at[me], small_send.at[0], gain_sem.at[0], dev)

    bits = []
    b = F // 2
    while b:
        bits.append(b)
        b //= 2
    top = len(bits)
    counts = [0]

    def forward(buf, sem, n, slot, dev):
        block = buf.at[slot, rows_of(n)]
        send(block, block, relay_send.at[0], sem.at[n, slot], dev)
        counts[0] += chunks[n][1]

    def arrived(buf, sem, n, slot):
        await_bytes(buf.at[slot, rows_of(n)], sem.at[n, slot])

    def stage(r):
        return 0 if r == 0 else len(bits) - ((r & -r).bit_length() - 1)

    def hop(buf, sem, n, lv, dts, ups=every, down=True, over=()):
        for r in range(F):
            if stage(r) != lv:
                continue
            for dt in dts:
                slot = (f ^ r) * T + from_t[dt]
                arrived(buf, sem, n, slot)
                for b in bits:
                    if b < ((r & -r) or F) and (dt in ups if b == F // 2 else down):
                        forward(buf, sem, n, slot, at(k, f ^ b, t))
                if dt in over:
                    forward(buf, sem, n, slot, at(1 - k, f, t))

    def prepare(first):
        if not first:
            await_bytes(lng.at[pl.ds(0, G)], gain_sem.at[1])
            await_bytes(lnb.at[pl.ds(0, G)], gain_sem.at[2])
        for load in loads[4:]:
            load.wait()
        taps[...] = taps_ref[0].astype(jnp.float32)
        await_bytes(gains.at[pl.ds(0, G - 1)], gain_sem.at[0])
        for s in range(G):
            turn[s : s + 1, :] = gains[s]
        cols = turn[...].T
        for s in range(G):
            rows = pl.ds(s * C, C)
            wcat[rows, :] = (wcat[rows, :].astype(jnp.float32) * cols[:, s : s + 1]).astype(jnp.bfloat16)

    def moments(ref, n):
        R = chunks[n][1]
        turn[0:2, :] = jnp.sum(ref[n], axis=0)
        cols = turn[...].T
        mu = cols[0:R, 0:1] / D
        var = cols[0:R, 1:2] / D - mu * mu
        return mu, lax.rsqrt(var + layer_eps)

    def layer_end(n, slot, mu, rs):
        half = (cg[slot, rows_of(n)].astype(jnp.float32) - mu) * rs * lng[slot] + lnb[slot]
        hg[slot, rows_of(n)] = (
            sg[slot, rows_of(n)].astype(jnp.float32) + (half + half * jnp.tanh(half))
        ).astype(jnp.bfloat16)

    def enter(n, swapped):
        await_bytes(sin.at[n, pl.ds(0, G)], sin_sem.at[n])
        mu, rs = moments(sin, n)
        if swapped:
            keep[0, 0 : chunks[n][1], :] = jnp.broadcast_to(mu, (chunks[n][1], C))
            keep[1, 0 : chunks[n][1], :] = jnp.broadcast_to(rs, (chunks[n][1], C))
        for dt in (ENTER if len(ENTER) == T else every):
            slot = f * T + from_t[dt]
            if dt or not zrelay:
                arrived(cg, c_sem, n, slot)
            layer_end(n, slot, mu, rs)
            for b in bits:
                if not (swapped and dt == 0 and b == F // 2):
                    forward(hg, h_sem, n, slot, at(k, f ^ b, t))

    def enter_swapped(n):
        slot = (f ^ (F // 2)) * T + t
        arrived(cg, c_sem, n, slot)
        layer_end(n, slot, keep[0, 0 : chunks[n][1], :], keep[1, 0 : chunks[n][1], :])
        for b in bits[1:]:
            forward(hg, h_sem, n, slot, at(k, f ^ b, t))

    def spread(n):
        slot = f * T + t
        arrived(cg, c_sem, n, slot)
        for dz in zrelay:
            forward(cg, c_sem, n, slot, at(k, f, to_t[dz]))

    def project(n, buf):
        start, R = chunks[n]
        blocks = [buf[s, rows_of(n)] for s in range(G)]
        squares = jnp.zeros((R, C), jnp.float32)
        for xb in blocks:
            xf = xb.astype(jnp.float32)
            squares = squares + xf * xf
        scale = lax.rsqrt(jnp.sum(squares, axis=1, keepdims=True) / D + norm_eps)
        both = jnp.dot(jnp.concatenate(blocks, axis=1), wcat[...], preferred_element_type=jnp.float32) * scale
        j = start % LEN
        pad[head + j : head + j + R, :] = both[:, :C] * (0.5 + 0.5 * jnp.tanh(0.5 * both[:, C:]))
        step = 32 if R % 32 == 0 else R
        for r0 in range(0, R, step):
            acc = jnp.zeros((step, C), jnp.float32)
            for w in range(W):
                o = head - (W - 1) + w + j + r0
                acc = acc + pad[o : o + step, :] * taps[w : w + 1, :]
            conv_own[start + r0 : start + r0 + step, :] = acc
        conv = conv_own[start : start + R, :]
        lane = lax.broadcasted_iota(jnp.int32, (R, LEN), 1)
        s1 = jnp.sum(conv, axis=1, keepdims=True)
        s2 = jnp.sum(conv * conv, axis=1, keepdims=True)
        turn[0:R, :] = jnp.where(lane == 0, s1, jnp.where(lane == 1, s2, 0.0))
        return conv, turn[...].T[0:2, :]

    def pass_on(n, first, swapped):
        conv, stat = project(n, sg if first else hg)
        rows = rows_of(n)
        sout[n] = stat
        conv_out[rows, :] = conv.astype(jnp.bfloat16)
        for dt in SEND if len(SEND) == T else every:
            if dt not in zrelay:
                send(conv_out.at[rows], cg.at[me, rows], next_send.at[0], c_sem.at[n, me], at(k + 1, f, to_t[dt]))
        for dev in plane(k + 1):
            send(sout.at[n], sin.at[n, me], stat_send.at[0], sin_sem.at[n], dev)
        if swapped:
            send(conv_out.at[rows], side.at[rows], swap_send.at[0], side_sem.at[n], at(k, f ^ (F // 2), t))
        if not first:
            for tt in to_t:
                send(hg.at[me, rows], sg.at[me, rows], next_send.at[0], s_sem.at[n, me], at(k + 1, f, tt))

    def swap_on(n):
        rows = rows_of(n)
        await_bytes(side.at[rows], side_sem.at[n])
        slot = (f ^ (F // 2)) * T + t
        send(side.at[rows], cg.at[slot, rows], swap_send.at[0], c_sem.at[n, slot], at(k + 1, f, t))

    def last_stats(n, first):
        _, stat = project(n, sg if first else hg)
        sfin[n, me] = stat
        for dev in peers:
            send(sfin.at[n, me], sfin.at[n, me], stat_send.at[0], sfin_sem.at[n], dev)

    def finish(n, first):
        start, R = chunks[n]
        await_bytes(sfin.at[n, pl.ds(0, G - 1)], sfin_sem.at[n])
        mu, rs = moments(sfin, n)
        half = (conv_own[start : start + R, :] - mu) * rs * lgain_ref[...] + lshift_ref[...]
        stream = (sg if first else hg)[me, rows_of(n)]
        new = (stream.astype(jnp.float32) + (half + half * jnp.tanh(half))).astype(jnp.bfloat16)
        owner, i = start // own_rows, start % own_rows
        rows = pl.ds(i, R)
        if owner == P_ - 1:
            out_ref[rows, :] = new
        else:
            new_buf[rows_of(n), :] = new
            send(new_buf.at[rows_of(n)], out_ref.at[rows], back_send.at[0], out_sem.at[0], at(owner, f, t))

    def drain(rows, sem):
        full = sg.shape[1]
        while rows >= full:
            m = min(G, rows // full)
            await_bytes(sg.at[pl.ds(0, m)], sem)
            rows -= m * full
        if rows:
            await_bytes(sg.at[0, pl.ds(0, rows)], sem)

    def run(first, last):
        counts[0] = 0
        kk = 0 if first else 1
        ops = []
        for n, (start, size) in enumerate(chunks):
            own = not cross or start // own_rows == kk
            swapped = cross and F > 1 and start >= SWAP
            at_ = functools.partial(when, chunks, own_rows, cross, kk, n)
            x1 = XCARRY if cross else ()
            zero = (0,) if swapped else ()
            if first:
                if own:
                    ops.append((at_("S0"), functools.partial(hop, sg, s_sem, n, 0, every, over=every if cross else ())))
                else:
                    ups = tuple(d for d in every if d not in x1)
                    ops.append((at_("S0"), functools.partial(hop, sg, s_sem, n, 0, every, ups)))
                for lv in range(1, top + 1):
                    over = zero if own and lv == 1 else ()
                    ops.append((at_("S%d" % min(lv, 2)), functools.partial(hop, sg, s_sem, n, lv, every, over=over)))
            else:
                if cross and own:
                    ups = tuple(sorted(set(x1 + zero)))
                    ops.append((at_("S0"), functools.partial(hop, sg, s_sem, n, 0, every, ups, False, every)))
                    if ups:
                        ops.append((at_("S1"), functools.partial(hop, sg, s_sem, n, 1, ups, (), False, x1)))
                else:
                    ops.append((at_("S0"), functools.partial(hop, sg, s_sem, n, 0, every, (), False)))
                    if swapped:
                        ops.append((at_("S1"), functools.partial(hop, sg, s_sem, n, 1, (0,), (), False)))
                if zrelay:
                    ops.append((at_("C00"), functools.partial(spread, n)))
                ops.append((at_("ent"), functools.partial(enter, n, swapped)))
                if swapped:
                    ops.append((at_("ent2"), functools.partial(enter_swapped, n)))
                for lv in range(1, top + 1):
                    dts = every[1:] if swapped and lv == 1 else every
                    ops.append((at_("C%d" % min(lv, 2)), functools.partial(hop, hg, h_sem, n, lv, dts)))
            if n == 0:
                ops.append((at_("prep"), functools.partial(prepare, first)))
            if last:
                ops.append((at_("step"), functools.partial(last_stats, n, first)))
                ops.append((at_("fin"), functools.partial(finish, n, first)))
            else:
                ops.append((at_("step"), functools.partial(pass_on, n, first, swapped)))
                if swapped:
                    ops.append((at_("swap"), functools.partial(swap_on, n)))
        if cross:
            feed(kk, FEED, mine_of(kk))
        greet()
        if not last:
            for dev in plane(k + 1):
                send(lgain_ref, lng.at[me], small_send.at[1], gain_sem.at[1], dev)
                send(lshift_ref, lnb.at[me], small_send.at[1], gain_sem.at[2], dev)
        for _, op in sorted(ops, key=lambda op: op[0]):
            op()
        drain(counts[0], relay_send.at[0])
        total = sg.shape[1]
        await_bytes(gains.at[pl.ds(0, G - 1)], small_send.at[0])
        if last:
            await_bytes(sfin.at[:, pl.ds(0, G - 1)], stat_send.at[0])
            if P_ > 1:
                drain(total - own_rows, back_send.at[0])
        else:
            await_bytes(sin.at[:, pl.ds(0, G)], stat_send.at[0])
            await_bytes(lng.at[pl.ds(0, G)], small_send.at[1])
            await_bytes(lnb.at[pl.ds(0, G)], small_send.at[1])
            drain(total * (T - len(zrelay)), next_send.at[0])
            if cross and F > 1:
                drain(2 * sum(c[1] for c in chunks if c[0] >= SWAP), swap_send.at[0])
            if not first:
                drain(total * T, next_send.at[0])

    if not cross:
        for q in range(feeds):
            feed(q, range(1, T), mine)
            if P_ > 1:
                pl.when(k != q)(functools.partial(feed, q, [0], mine))
    if P_ == 1:
        run(True, True)
    else:
        pl.when(k == 0)(lambda: run(True, False))
        pl.when(k == P_ - 1)(lambda: run(False, True))
        if P_ > 2:
            pl.when((k > 0) & (k < P_ - 1))(lambda: run(False, False))

    drain(own_rows * (T - 1 if cross else feeds * T - 1), feed_send.at[0])
    if P_ > 2:
        pl.when(k >= feeds)(lambda: await_bytes(x_ref, feed_send.at[0]))
    if P_ > 1:
        pl.when(k < P_ - 1)(lambda: await_bytes(out_ref, out_sem.at[0]))


def plan(sizes, own_rows):
    if sizes[0] == 2 and sizes[2] & (sizes[2] - 1) == 0 and all(sum(split) == own_rows for split in SPLITS):
        rows = [size for split in SPLITS for size in split]
        return [(sum(rows[:i]), size) for i, size in enumerate(rows)], True
    size = min(64, own_rows)
    return [(i * size, size) for i in range(own_rows * sizes[0] // size)], False


def when(chunks, own_rows, cross, kk, n, op):
    if cross and TIMES:
        return TIMES[kk][op][n] if op != "prep" else TIMES[kk]["step"][0] - 0.01
    start, size = chunks[n]
    late = start + size
    mine = late - start // own_rows * own_rows if cross else late
    own = not cross or start // own_rows == kk
    base = 6.6 + 1.4 * late / 64
    s0 = 3 + 0.7 * mine / 64 if own else 5.5 + 0.7 * mine / 64
    s1 = 5.5 + 1.4 * mine / 64 if own else 11.5 + 0.8 * mine / 64
    first = {"S0": s0, "S1": s1, "S2": s1 + 1, "step": s1 + 1.1, "prep": s1 + 1.05, "swap": s1 + 4, "fin": s1 + 6}
    later = {
        "S0": s0, "S1": s1, "C00": base + 3, "ent": base + 6, "ent2": base + 8, "C1": base + 9, "C2": base + 10,
        "prep": base + 5.9, "step": base + 10.1, "swap": base + 13, "fin": base + 15,
    }
    return (later if kk else first)[op]


def local(sizes, inputs, norm_gain, w_value, w_gate, w_taps, ln_gain, ln_shift):
    P_, F, T = sizes
    G = F * T
    own_rows, C = inputs.shape
    TOK = own_rows * P_
    chunks, _ = plan(sizes, own_rows)
    NC = len(chunks)
    D = w_value.shape[1]
    W = w_taps.shape[1]
    head = -(-(W - 1) // 8) * 8
    operands = (inputs, norm_gain, w_value, w_gate, w_taps, ln_gain, ln_shift)
    dma = pltpu.SemaphoreType.DMA
    f32, bf16 = jnp.float32, jnp.bfloat16
    V = pltpu.VMEM
    return pl.pallas_call(
        functools.partial(kernel, sizes),
        out_shape=pltpu.VMEM((own_rows, C), bf16),
        in_specs=[pl.BlockSpec(memory_space=pl.ANY)] * 7,
        out_specs=pl.BlockSpec(memory_space=pltpu.VMEM),
        scratch_shapes=[
            V(inputs.shape, bf16), V(norm_gain.shape, bf16), V((D, 2 * C), bf16), V(w_taps.shape, bf16),
            V(ln_gain.shape, f32), V(ln_shift.shape, f32),
            dma((len(operands),)),
            V((G, TOK, C), bf16), V((G, TOK, C), bf16), V((G, TOK, C), bf16),
            V((G, 1, C), f32), V((G, 1, C), f32), V((G, 1, C), f32),
            V((NC, G, 2, LEN), f32), V((NC, G, 2, LEN), f32), V((NC, 2, LEN), f32),
            V((LEN + head, C), f32), V((W, C), f32),
            V((TOK, C), f32), V((TOK, C), bf16), V((2, LEN, C), f32), V((TOK, C), bf16),
            V((LEN, LEN), f32),
            dma((NC, G)), dma((NC, G)), dma((NC, G)), dma((NC,)), dma((NC,)), dma((3,)), dma((1,)),
            dma((1,)), dma((1,)), dma((2,)), dma((1,)), dma((1,)), dma((1,)),
            V((TOK, C), bf16), dma((NC,)), dma((1,)),
        ],
        compiler_params=pltpu.CompilerParams(collective_id=0, has_side_effects=True),
    )(*operands)


def solution(mesh):
    sizes = (mesh.shape["pp"], mesh.shape["fs"], mesh.shape["tp"])
    in_specs = (
        P("pp", ("fs", "tp")),
        P("pp", ("fs", "tp")),
        P("pp", None, ("fs", "tp")),
        P("pp", None, ("fs", "tp")),
        P("pp", None, ("fs", "tp")),
        P("pp", ("fs", "tp")),
        P("pp", ("fs", "tp")),
    )
    out_specs = P("pp", ("fs", "tp"))
    return jax.shard_map(
        functools.partial(local, sizes), mesh=mesh, in_specs=in_specs, out_specs=out_specs,
        check_vma=False,
    )
```

time: 62.2 us -> 46.2 us (0.74)
  Pallas kernels: 60.5 us -> 45.4 us
  local copies, waits for them, and re-layouts: 1.47 us -> 0.63 us
    pallas_call x1, Pallas kernels: 60.5 us -> 45.4 us  [local(): pl.pallas_call(functools.partial(kernel, sizes), out_shape=pltpu.VMEM((ow...]
    unnamed x1, local copies, waits for them, and re-layouts: 1.47 us -> 0.63 us
where the time goes in v2:
time: 46.2 us; the launch traced here: 46 us
  Pallas kernels  45.4 us (98%)
  local copies, waits for them, and re-layouts  0.63 us (1%)
    pallas_call x1, Pallas kernels, local(): pl.pallas_call(functools.partial(kernel, sizes), out_shape=pltpu.VMEM((ow...  45.4 us

profile of v2, /device:TPU:3, one launch (start us, length us, event | category | flops | bytes accessed | tf_op | source)
XLA Modules:
  0.0 46.0 jit_solution(11792996079421271218)
XLA Ops:
  0.0 45.4 %shard_map.73 = bf16[256,128]{1,0:T(8,128)(2,1)S(1)} custom-call(bf16[256,128]{1,0:T(8,128)(2,1)} %x_hbm.1, bf16[1,128]{1,0:T(2,128)(2,1)} %gain_hbm.1, bf16[1,2048,128]{2,1,0:T(8,128)(2,1)} %wv_hbm.1, bf16[1,2048,128]{2,1,0:T(8,128)(2,1)} %wg_hbm.1, bf16[1,31,128]{2,1,0:T(8,128)(2,1)} %taps_hbm.1, f32[1,128]{1,0:T(1,128)} %lgain_hbm.1, f32[1,128]{1,0:T(1,128)} %lshift_hbm.1), custom_call_target="tpu_custom_call" | custom-call | tf_op jit(solution)/shard_map/pallas_call | solution.py:476
  45.4 0.6 %copy.9 = bf16[256,128]{1,0:T(8,128)(2,1)} copy(bf16[256,128]{1,0:T(8,128)(2,1)S(1)} %shard_map.73) | data formatting | bytes 131072

commit v3 on v2

--- a/solution.py
+++ b/solution.py
@@ -10,12 +10,15 @@
 LEN = 128
 SPLITS = ((128, 128), (128, 128))
 FEED = (2, 3, 1)
-SEND = (3, 2, 1, 0)
+SEND = (0, 3, 2, 1)
 ENTER = (0, 1, 3, 2)
-XCARRY = (1, 2)
+XCARRY = (1, 2, 3)
 ZRELAY = (1, 2)
 SWAP = 256
-TIMES = ()
+TIMES = (
+    {"S0": (-0.48, 4.35, 10.17, 11.39), "S1": (6.67, 11.13, 17.25, 20.33), "S2": (8.5, 15.39, 18.61, 20.55), "step": (8.5, 15.39, 18.61, 20.55), "swap": (0, 0, 31.88, 26.88)},
+    {"S0": (10.67, 16.26, 7.57, 7.57), "C00": (16.08, 17.31, 18.47, 19.95), "ent": (18.0, 19.3, 21.72, 24.23), "C1": (21.04, 25.35, 26.83, 31.69), "C2": (21.81, 26.26, 31.37, 33.41), "step": (21.81, 26.27, 31.37, 33.42), "fin": (32.83, 34.11, 38.98, 44.31), "S1": (0, 0, 8.63, 11.78), "ent2": (0, 0, 29.86, 28.1)},
+)
 
 
 norm_eps = 1e-06
@@ -72,6 +75,7 @@
     side,
     side_sem,
     swap_send,
+    meet_sem,
 ):
     P_, F, T = sizes
     G = F * T
@@ -120,6 +124,11 @@
     def plane(kk):
         return [at(kk, lax.rem(f + df, F), to_t[dt]) for dt in range(T - 1, -1, -1) for df in range(F)]
 
+    bits = []
+    b = F // 2
+    while b:
+        bits.append(b)
+        b //= 2
     pow2 = T & (T - 1) == 0
     every = tuple(range(T))
     chunks, cross = plan(sizes, own_rows)
@@ -159,7 +168,11 @@
         else:
             own_copies(mine)
     barrier = pltpu.get_barrier_semaphore()
-    everyone = peers + [dev for dk in range(1, P_) for dev in plane(lax.rem(k + dk, P_))]
+    column = [at(k, f, tt) for tt in to_t[1:]]
+    if cross:
+        everyone = column + [at(k, f ^ b, t) for b in bits] + [at(1 - k, f, t)]
+    else:
+        everyone = peers + [dev for dk in range(1, P_) for dev in plane(lax.rem(k + dk, P_))]
     for dev in everyone:
         pl.semaphore_signal(barrier, inc=1, device_id=dev, device_id_type=MESH)
     for load in loads[:4]:
@@ -171,15 +184,20 @@
     turn[...] = jnp.zeros_like(turn)
     pl.semaphore_wait(barrier, len(everyone))
 
+    def meet():
+        for i, b in enumerate(bits):
+            pl.semaphore_signal(meet_sem.at[i], inc=1, device_id=at(k, f ^ b, t), device_id_type=MESH)
+            pl.semaphore_wait(meet_sem.at[i], 1)
+        pl.semaphore_signal(meet_sem.at[top], inc=1, device_id=at(1 - k, f, t), device_id_type=MESH)
+
+    def give(n, i, start, size, dev):
+        send(x_ref.at[pl.ds(i, size)], sg.at[me, pl.ds(start, size)], relay_send.at[0], s_sem.at[n, me], dev)
+        counts[0] += size
+
     def greet():
         for dev in peers:
             send(gains.at[me], gains.at[me], small_send.at[0], gain_sem.at[0], dev)
 
-    bits = []
-    b = F // 2
-    while b:
-        bits.append(b)
-        b //= 2
     top = len(bits)
     counts = [0]
 
@@ -194,13 +212,15 @@
     def stage(r):
         return 0 if r == 0 else len(bits) - ((r & -r).bit_length() - 1)
 
-    def hop(buf, sem, n, lv, dts, ups=every, down=True, over=()):
+    def hop(buf, sem, n, lv, dts, ups=every, down=True, over=(), given=False):
         for r in range(F):
             if stage(r) != lv:
                 continue
             for dt in dts:
                 slot = (f ^ r) * T + from_t[dt]
                 arrived(buf, sem, n, slot)
+                if given and dt == 0:
+                    continue
                 for b in bits:
                     if b < ((r & -r) or F) and (dt in ups if b == F // 2 else down):
                         forward(buf, sem, n, slot, at(k, f ^ b, t))
@@ -240,8 +260,8 @@
         await_bytes(sin.at[n, pl.ds(0, G)], sin_sem.at[n])
         mu, rs = moments(sin, n)
         if swapped:
-            keep[0, 0 : chunks[n][1], :] = jnp.broadcast_to(mu, (chunks[n][1], C))
-            keep[1, 0 : chunks[n][1], :] = jnp.broadcast_to(rs, (chunks[n][1], C))
+            keep[n, 0, 0 : chunks[n][1], :] = jnp.broadcast_to(mu, (chunks[n][1], C))
+            keep[n, 1, 0 : chunks[n][1], :] = jnp.broadcast_to(rs, (chunks[n][1], C))
         for dt in (ENTER if len(ENTER) == T else every):
             slot = f * T + from_t[dt]
             if dt or not zrelay:
@@ -254,7 +274,7 @@
     def enter_swapped(n):
         slot = (f ^ (F // 2)) * T + t
         arrived(cg, c_sem, n, slot)
-        layer_end(n, slot, keep[0, 0 : chunks[n][1], :], keep[1, 0 : chunks[n][1], :])
+        layer_end(n, slot, keep[n, 0, 0 : chunks[n][1], :], keep[n, 1, 0 : chunks[n][1], :])
         for b in bits[1:]:
             forward(hg, h_sem, n, slot, at(k, f ^ b, t))
 
@@ -294,11 +314,11 @@
         rows = rows_of(n)
         sout[n] = stat
         conv_out[rows, :] = conv.astype(jnp.bfloat16)
+        for dev in plane(k + 1):
+            send(sout.at[n], sin.at[n, me], stat_send.at[0], sin_sem.at[n], dev)
         for dt in SEND if len(SEND) == T else every:
             if dt not in zrelay:
                 send(conv_out.at[rows], cg.at[me, rows], next_send.at[0], c_sem.at[n, me], at(k + 1, f, to_t[dt]))
-        for dev in plane(k + 1):
-            send(sout.at[n], sin.at[n, me], stat_send.at[0], sin_sem.at[n], dev)
         if swapped:
             send(conv_out.at[rows], side.at[rows], swap_send.at[0], side_sem.at[n], at(k, f ^ (F // 2), t))
         if not first:
@@ -353,7 +373,7 @@
             zero = (0,) if swapped else ()
             if first:
                 if own:
-                    ops.append((at_("S0"), functools.partial(hop, sg, s_sem, n, 0, every, over=every if cross else ())))
+                    ops.append((at_("S0"), functools.partial(hop, sg, s_sem, n, 0, every, over=every if cross else (), given=cross)))
                 else:
                     ups = tuple(d for d in every if d not in x1)
                     ops.append((at_("S0"), functools.partial(hop, sg, s_sem, n, 0, every, ups)))
@@ -363,7 +383,7 @@
             else:
                 if cross and own:
                     ups = tuple(sorted(set(x1 + zero)))
-                    ops.append((at_("S0"), functools.partial(hop, sg, s_sem, n, 0, every, ups, False, every)))
+                    ops.append((at_("S0"), functools.partial(hop, sg, s_sem, n, 0, every, ups, False, every, True)))
                     if ups:
                         ops.append((at_("S1"), functools.partial(hop, sg, s_sem, n, 1, ups, (), False, x1)))
                 else:
@@ -388,8 +408,19 @@
                 if swapped:
                     ops.append((at_("swap"), functools.partial(swap_on, n)))
         if cross:
-            feed(kk, FEED, mine_of(kk))
+            for entry in mine_of(kk):
+                feed(kk, FEED, [entry])
+                n, start, i = entry
+                size = chunks[n][1]
+                swapped = start >= SWAP
+                for b in bits:
+                    if (first or 0 in XCARRY or swapped) if b == F // 2 else first:
+                        give(n, i, start, size, at(k, f ^ b, t))
+                give(n, i, start, size, at(1 - k, f, t))
+            meet()
         greet()
+        if cross:
+            pl.semaphore_wait(meet_sem.at[top], 1)
         if not last:
             for dev in plane(k + 1):
                 send(lgain_ref, lng.at[me], small_send.at[1], gain_sem.at[1], dev)
@@ -443,7 +474,9 @@
 
 def when(chunks, own_rows, cross, kk, n, op):
     if cross and TIMES:
-        return TIMES[kk][op][n] if op != "prep" else TIMES[kk]["step"][0] - 0.01
+        if op == "prep":
+            return TIMES[kk]["C00" if kk else "step"][0] - 0.01
+        return TIMES[kk][op][n]
     start, size = chunks[n]
     late = start + size
     mine = late - start // own_rows * own_rows if cross else late
@@ -454,7 +487,7 @@
     first = {"S0": s0, "S1": s1, "S2": s1 + 1, "step": s1 + 1.1, "prep": s1 + 1.05, "swap": s1 + 4, "fin": s1 + 6}
     later = {
         "S0": s0, "S1": s1, "C00": base + 3, "ent": base + 6, "ent2": base + 8, "C1": base + 9, "C2": base + 10,
-        "prep": base + 5.9, "step": base + 10.1, "swap": base + 13, "fin": base + 15,
+        "prep": base + 2.9, "step": base + 10.1, "swap": base + 13, "fin": base + 15,
     }
     return (later if kk else first)[op]
 
@@ -486,11 +519,11 @@
             V((G, 1, C), f32), V((G, 1, C), f32), V((G, 1, C), f32),
             V((NC, G, 2, LEN), f32), V((NC, G, 2, LEN), f32), V((NC, 2, LEN), f32),
             V((LEN + head, C), f32), V((W, C), f32),
-            V((TOK, C), f32), V((TOK, C), bf16), V((2, LEN, C), f32), V((TOK, C), bf16),
+            V((TOK, C), f32), V((TOK, C), bf16), V((NC, 2, LEN, C), f32), V((TOK, C), bf16),
             V((LEN, LEN), f32),
             dma((NC, G)), dma((NC, G)), dma((NC, G)), dma((NC,)), dma((NC,)), dma((3,)), dma((1,)),
             dma((1,)), dma((1,)), dma((2,)), dma((1,)), dma((1,)), dma((1,)),
-            V((TOK, C), bf16), dma((NC,)), dma((1,)),
+            V((TOK, C), bf16), dma((NC,)), dma((1,)), pltpu.SemaphoreType.REGULAR((8,)),
         ],
         compiler_params=pltpu.CompilerParams(collective_id=0, has_side_effects=True),
     )(*operands)

time: 46.2 us -> 41.8 us (0.905)
  the two profiles are of different devices: /device:TPU:3 before, /device:TPU:0 now
where the time goes in v3:
time: 41.8 us; the launch traced here: 41.7 us
  Pallas kernels  41 us (98%)
  local copies, waits for them, and re-layouts  0.63 us (2%)
    pallas_call x1, Pallas kernels, local(): pl.pallas_call(functools.partial(kernel, sizes), out_shape=pltpu.VMEM((ow...  41 us

profile of v3, /device:TPU:0, one launch (start us, length us, event | category | flops | bytes accessed | tf_op | source)
XLA Modules:
  0.0 41.7 jit_solution(8821102842824800041)
XLA Ops:
  0.0 41.0 %shard_map.73 = bf16[256,128]{1,0:T(8,128)(2,1)S(1)} custom-call(bf16[256,128]{1,0:T(8,128)(2,1)} %x_hbm.1, bf16[1,128]{1,0:T(2,128)(2,1)} %gain_hbm.1, bf16[1,2048,128]{2,1,0:T(8,128)(2,1)} %wv_hbm.1, bf16[1,2048,128]{2,1,0:T(8,128)(2,1)} %wg_hbm.1, bf16[1,31,128]{2,1,0:T(8,128)(2,1)} %taps_hbm.1, f32[1,128]{1,0:T(1,128)} %lgain_hbm.1, f32[1,128]{1,0:T(1,128)} %lshift_hbm.1), custom_call_target="tpu_custom_call" | custom-call | tf_op jit(solution)/shard_map/pallas_call | solution.py:509
  41.0 0.6 %copy.9 = bf16[256,128]{1,0:T(8,128)(2,1)} copy(bf16[256,128]{1,0:T(8,128)(2,1)S(1)} %shard_map.73) | data formatting | bytes 131072

commit v4 on v3

--- a/solution.py
+++ b/solution.py
@@ -48,7 +48,6 @@
     hg,
     gains,
     lng,
-    lnb,
     sin,
     sfin,
     sout,
@@ -57,6 +56,7 @@
     conv_own,
     conv_out,
     keep,
+    lnp,
     new_buf,
     turn,
     s_sem,
@@ -66,15 +66,9 @@
     sfin_sem,
     gain_sem,
     out_sem,
-    feed_send,
-    relay_send,
-    small_send,
-    stat_send,
-    next_send,
-    back_send,
+    sent,
     side,
     side_sem,
-    swap_send,
     meet_sem,
 ):
     P_, F, T = sizes
@@ -143,7 +137,7 @@
             size = chunks[n][1] if cross else chunks[0][1]
             for dt in dts:
                 send(
-                    x_ref.at[pl.ds(i, size)], sg.at[me, pl.ds(start, size)], feed_send.at[0], s_sem.at[n, me],
+                    x_ref.at[pl.ds(i, size)], sg.at[me, pl.ds(start, size)], sent.at[0], s_sem.at[n, dt],
                     at(q, f, to_t[dt]),
                 )
 
@@ -151,7 +145,7 @@
         for n, start, i in mine:
             size = chunks[n][1] if cross else chunks[0][1]
             pltpu.make_async_copy(
-                x_hbm.at[pl.ds(i, size)], sg.at[me, pl.ds(start, size)], s_sem.at[n, me]
+                x_hbm.at[pl.ds(i, size)], sg.at[me, pl.ds(start, size)], s_sem.at[n, 0]
             ).start()
 
     def mine_of(kk):
@@ -178,8 +172,8 @@
     for load in loads[:4]:
         load.wait()
     gains[me] = gain_ref[...].astype(jnp.float32)
-    lgain_ref[...] = lgain_ref[...] * 0.5
-    lshift_ref[...] = lshift_ref[...] * 0.5
+    lnp[0] = lgain_ref[...] * 0.5
+    lnp[1] = lshift_ref[...] * 0.5
     pad[0:head, :] = jnp.zeros((head, C), jnp.float32)
     turn[...] = jnp.zeros_like(turn)
     pl.semaphore_wait(barrier, len(everyone))
@@ -190,47 +184,57 @@
             pl.semaphore_wait(meet_sem.at[i], 1)
         pl.semaphore_signal(meet_sem.at[top], inc=1, device_id=at(1 - k, f, t), device_id_type=MESH)
 
-    def give(n, i, start, size, dev):
-        send(x_ref.at[pl.ds(i, size)], sg.at[me, pl.ds(start, size)], relay_send.at[0], s_sem.at[n, me], dev)
+    def give(n, i, start, size, cls, dev):
+        send(x_ref.at[pl.ds(i, size)], sg.at[me, pl.ds(start, size)], sent.at[0], s_sem.at[n, cls], dev)
         counts[0] += size
 
     def greet():
         for dev in peers:
-            send(gains.at[me], gains.at[me], small_send.at[0], gain_sem.at[0], dev)
+            send(gains.at[me], gains.at[me], sent.at[0], gain_sem.at[0], dev)
 
     top = len(bits)
     counts = [0]
 
-    def forward(buf, sem, n, slot, dev):
-        block = buf.at[slot, rows_of(n)]
-        send(block, block, relay_send.at[0], sem.at[n, slot], dev)
-        counts[0] += chunks[n][1]
-
-    def arrived(buf, sem, n, slot):
-        await_bytes(buf.at[slot, rows_of(n)], sem.at[n, slot])
-
     def stage(r):
         return 0 if r == 0 else len(bits) - ((r & -r).bit_length() - 1)
 
-    def hop(buf, sem, n, lv, dts, ups=every, down=True, over=(), given=False):
+    relayed = [r for r in range(F) if not top or stage(r) < top]
+    ends = [r for r in range(F) if r not in relayed]
+
+    def kind(r, dt):
+        if top and stage(r) == top:
+            return len(relayed) * T
+        return relayed.index(r) * T + dt
+
+    def forward(buf, sem, n, slot, cls, dev):
+        block = buf.at[slot, rows_of(n)]
+        send(block, block, sent.at[0], sem.at[n, cls], dev)
+        counts[0] += chunks[n][1]
+
+    def arrived(buf, sem, n, slot, cls):
+        await_bytes(buf.at[slot, rows_of(n)], sem.at[n, cls])
+
+    def hop(buf, sem, n, lv, dts, ups=every, down=True, over=(), given=False, base=0):
+        if top and lv == top:
+            await_bytes(buf.at[pl.ds(0, len(ends) * T), rows_of(n)], sem.at[n, kind(ends[0], 0) - base])
+            return
         for r in range(F):
             if stage(r) != lv:
                 continue
             for dt in dts:
                 slot = (f ^ r) * T + from_t[dt]
-                arrived(buf, sem, n, slot)
+                arrived(buf, sem, n, slot, kind(r, dt) - base)
                 if given and dt == 0:
                     continue
                 for b in bits:
                     if b < ((r & -r) or F) and (dt in ups if b == F // 2 else down):
-                        forward(buf, sem, n, slot, at(k, f ^ b, t))
+                        forward(buf, sem, n, slot, kind(r ^ b, dt) - base, at(k, f ^ b, t))
                 if dt in over:
-                    forward(buf, sem, n, slot, at(1 - k, f, t))
+                    forward(buf, sem, n, slot, kind(r, dt) - base, at(1 - k, f, t))
 
     def prepare(first):
         if not first:
             await_bytes(lng.at[pl.ds(0, G)], gain_sem.at[1])
-            await_bytes(lnb.at[pl.ds(0, G)], gain_sem.at[2])
         for load in loads[4:]:
             load.wait()
         taps[...] = taps_ref[0].astype(jnp.float32)
@@ -251,7 +255,7 @@
         return mu, lax.rsqrt(var + layer_eps)
 
     def layer_end(n, slot, mu, rs):
-        half = (cg[slot, rows_of(n)].astype(jnp.float32) - mu) * rs * lng[slot] + lnb[slot]
+        half = (cg[slot, rows_of(n)].astype(jnp.float32) - mu) * rs * lng[slot, 0] + lng[slot, 1]
         hg[slot, rows_of(n)] = (
             sg[slot, rows_of(n)].astype(jnp.float32) + (half + half * jnp.tanh(half))
         ).astype(jnp.bfloat16)
@@ -265,24 +269,24 @@
         for dt in (ENTER if len(ENTER) == T else every):
             slot = f * T + from_t[dt]
             if dt or not zrelay:
-                arrived(cg, c_sem, n, slot)
+                arrived(cg, c_sem, n, slot, dt)
             layer_end(n, slot, mu, rs)
             for b in bits:
                 if not (swapped and dt == 0 and b == F // 2):
-                    forward(hg, h_sem, n, slot, at(k, f ^ b, t))
+                    forward(hg, h_sem, n, slot, kind(b, dt) - T, at(k, f ^ b, t))
 
     def enter_swapped(n):
         slot = (f ^ (F // 2)) * T + t
-        arrived(cg, c_sem, n, slot)
+        arrived(cg, c_sem, n, slot, T)
         layer_end(n, slot, keep[n, 0, 0 : chunks[n][1], :], keep[n, 1, 0 : chunks[n][1], :])
         for b in bits[1:]:
-            forward(hg, h_sem, n, slot, at(k, f ^ b, t))
+            forward(hg, h_sem, n, slot, kind(F // 2 ^ b, 0) - T, at(k, f ^ b, t))
 
     def spread(n):
         slot = f * T + t
-        arrived(cg, c_sem, n, slot)
+        arrived(cg, c_sem, n, slot, 0)
         for dz in zrelay:
-            forward(cg, c_sem, n, slot, at(k, f, to_t[dz]))
+            forward(cg, c_sem, n, slot, dz, at(k, f, to_t[dz]))
 
     def project(n, buf):
         start, R = chunks[n]
@@ -315,33 +319,33 @@
         sout[n] = stat
         conv_out[rows, :] = conv.astype(jnp.bfloat16)
         for dev in plane(k + 1):
-            send(sout.at[n], sin.at[n, me], stat_send.at[0], sin_sem.at[n], dev)
+            send(sout.at[n], sin.at[n, me], sent.at[0], sin_sem.at[n], dev)
         for dt in SEND if len(SEND) == T else every:
             if dt not in zrelay:
-                send(conv_out.at[rows], cg.at[me, rows], next_send.at[0], c_sem.at[n, me], at(k + 1, f, to_t[dt]))
+                send(conv_out.at[rows], cg.at[me, rows], sent.at[0], c_sem.at[n, dt], at(k + 1, f, to_t[dt]))
         if swapped:
-            send(conv_out.at[rows], side.at[rows], swap_send.at[0], side_sem.at[n], at(k, f ^ (F // 2), t))
+            send(conv_out.at[rows], side.at[rows], sent.at[0], side_sem.at[n], at(k, f ^ (F // 2), t))
         if not first:
-            for tt in to_t:
-                send(hg.at[me, rows], sg.at[me, rows], next_send.at[0], s_sem.at[n, me], at(k + 1, f, tt))
+            for dt in every:
+                send(hg.at[me, rows], sg.at[me, rows], sent.at[0], s_sem.at[n, dt], at(k + 1, f, to_t[dt]))
 
     def swap_on(n):
         rows = rows_of(n)
         await_bytes(side.at[rows], side_sem.at[n])
         slot = (f ^ (F // 2)) * T + t
-        send(side.at[rows], cg.at[slot, rows], swap_send.at[0], c_sem.at[n, slot], at(k + 1, f, t))
+        send(side.at[rows], cg.at[slot, rows], sent.at[0], c_sem.at[n, T], at(k + 1, f, t))
 
     def last_stats(n, first):
         _, stat = project(n, sg if first else hg)
         sfin[n, me] = stat
         for dev in peers:
-            send(sfin.at[n, me], sfin.at[n, me], stat_send.at[0], sfin_sem.at[n], dev)
+            send(sfin.at[n, me], sfin.at[n, me], sent.at[0], sfin_sem.at[n], dev)
 
     def finish(n, first):
         start, R = chunks[n]
         await_bytes(sfin.at[n, pl.ds(0, G - 1)], sfin_sem.at[n])
         mu, rs = moments(sfin, n)
-        half = (conv_own[start : start + R, :] - mu) * rs * lgain_ref[...] + lshift_ref[...]
+        half = (conv_own[start : start + R, :] - mu) * rs * lnp[0] + lnp[1]
         stream = (sg if first else hg)[me, rows_of(n)]
         new = (stream.astype(jnp.float32) + (half + half * jnp.tanh(half))).astype(jnp.bfloat16)
         owner, i = start // own_rows, start % own_rows
@@ -350,7 +354,7 @@
             out_ref[rows, :] = new
         else:
             new_buf[rows_of(n), :] = new
-            send(new_buf.at[rows_of(n)], out_ref.at[rows], back_send.at[0], out_sem.at[0], at(owner, f, t))
+            send(new_buf.at[rows_of(n)], out_ref.at[rows], sent.at[0], out_sem.at[0], at(owner, f, t))
 
     def drain(rows, sem):
         full = sg.shape[1]
@@ -397,7 +401,7 @@
                     ops.append((at_("ent2"), functools.partial(enter_swapped, n)))
                 for lv in range(1, top + 1):
                     dts = every[1:] if swapped and lv == 1 else every
-                    ops.append((at_("C%d" % min(lv, 2)), functools.partial(hop, hg, h_sem, n, lv, dts)))
+                    ops.append((at_("C%d" % min(lv, 2)), functools.partial(hop, hg, h_sem, n, lv, dts, base=T)))
             if n == 0:
                 ops.append((at_("prep"), functools.partial(prepare, first)))
             if last:
@@ -415,34 +419,32 @@
                 swapped = start >= SWAP
                 for b in bits:
                     if (first or 0 in XCARRY or swapped) if b == F // 2 else first:
-                        give(n, i, start, size, at(k, f ^ b, t))
-                give(n, i, start, size, at(1 - k, f, t))
+                        give(n, i, start, size, kind(b, 0), at(k, f ^ b, t))
+                give(n, i, start, size, 0, at(1 - k, f, t))
             meet()
         greet()
         if cross:
             pl.semaphore_wait(meet_sem.at[top], 1)
         if not last:
             for dev in plane(k + 1):
-                send(lgain_ref, lng.at[me], small_send.at[1], gain_sem.at[1], dev)
-                send(lshift_ref, lnb.at[me], small_send.at[1], gain_sem.at[2], dev)
+                send(lnp, lng.at[me], sent.at[0], gain_sem.at[1], dev)
         for _, op in sorted(ops, key=lambda op: op[0]):
             op()
-        drain(counts[0], relay_send.at[0])
+        drain(counts[0], sent.at[0])
         total = sg.shape[1]
-        await_bytes(gains.at[pl.ds(0, G - 1)], small_send.at[0])
+        await_bytes(gains.at[pl.ds(0, G - 1)], sent.at[0])
         if last:
-            await_bytes(sfin.at[:, pl.ds(0, G - 1)], stat_send.at[0])
+            await_bytes(sfin.at[:, pl.ds(0, G - 1)], sent.at[0])
             if P_ > 1:
-                drain(total - own_rows, back_send.at[0])
+                drain(total - own_rows, sent.at[0])
         else:
-            await_bytes(sin.at[:, pl.ds(0, G)], stat_send.at[0])
-            await_bytes(lng.at[pl.ds(0, G)], small_send.at[1])
-            await_bytes(lnb.at[pl.ds(0, G)], small_send.at[1])
-            drain(total * (T - len(zrelay)), next_send.at[0])
+            await_bytes(sin.at[:, pl.ds(0, G)], sent.at[0])
+            await_bytes(lng.at[pl.ds(0, G)], sent.at[0])
+            drain(total * (T - len(zrelay)), sent.at[0])
             if cross and F > 1:
-                drain(2 * sum(c[1] for c in chunks if c[0] >= SWAP), swap_send.at[0])
+                drain(2 * sum(c[1] for c in chunks if c[0] >= SWAP), sent.at[0])
             if not first:
-                drain(total * T, next_send.at[0])
+                drain(total * T, sent.at[0])
 
     if not cross:
         for q in range(feeds):
@@ -457,9 +459,9 @@
         if P_ > 2:
             pl.when((k > 0) & (k < P_ - 1))(lambda: run(False, False))
 
-    drain(own_rows * (T - 1 if cross else feeds * T - 1), feed_send.at[0])
+    drain(own_rows * (T - 1 if cross else feeds * T - 1), sent.at[0])
     if P_ > 2:
-        pl.when(k >= feeds)(lambda: await_bytes(x_ref, feed_send.at[0]))
+        pl.when(k >= feeds)(lambda: await_bytes(x_ref, sent.at[0]))
     if P_ > 1:
         pl.when(k < P_ - 1)(lambda: await_bytes(out_ref, out_sem.at[0]))
 
@@ -516,14 +518,14 @@
             V(ln_gain.shape, f32), V(ln_shift.shape, f32),
             dma((len(operands),)),
             V((G, TOK, C), bf16), V((G, TOK, C), bf16), V((G, TOK, C), bf16),
-            V((G, 1, C), f32), V((G, 1, C), f32), V((G, 1, C), f32),
+            V((G, 1, C), f32), V((G, 2, 1, C), f32),
             V((NC, G, 2, LEN), f32), V((NC, G, 2, LEN), f32), V((NC, 2, LEN), f32),
             V((LEN + head, C), f32), V((W, C), f32),
-            V((TOK, C), f32), V((TOK, C), bf16), V((NC, 2, LEN, C), f32), V((TOK, C), bf16),
+            V((TOK, C), f32), V((TOK, C), bf16), V((NC, 2, LEN, C), f32), V((2, 1, C), f32), V((TOK, C), bf16),
             V((LEN, LEN), f32),
-            dma((NC, G)), dma((NC, G)), dma((NC, G)), dma((NC,)), dma((NC,)), dma((3,)), dma((1,)),
-            dma((1,)), dma((1,)), dma((2,)), dma((1,)), dma((1,)), dma((1,)),
-            V((TOK, C), bf16), dma((NC,)), dma((1,)), pltpu.SemaphoreType.REGULAR((8,)),
+            dma((NC, T * F)) if F & (F - 1) else dma((NC, max(F // 2, 1) * T + 1)),
+            dma((NC, T + 1)), dma((NC, max(F // 2 - 1, 0) * T + 1)), dma((NC,)), dma((NC,)), dma((2,)), dma((1,)),
+            dma((1,)), V((TOK, C), bf16), dma((NC,)), pltpu.SemaphoreType.REGULAR((4,)),
         ],
         compiler_params=pltpu.CompilerParams(collective_id=0, has_side_effects=True),
     )(*operands)

time: 41.8 us -> 40.2 us (0.962)
  the two profiles are of different devices: /device:TPU:0 before, /device:TPU:3 now
where the time goes in v4:
time: 40.2 us; the launch traced here: 39.6 us
  Pallas kernels  39 us (97%)
  local copies, waits for them, and re-layouts  0.63 us (2%)
    pallas_call x1, Pallas kernels, local(): pl.pallas_call(functools.partial(kernel, sizes), out_shape=pltpu.VMEM((ow...  39 us

profile of v4, /device:TPU:3, one launch (start us, length us, event | category | flops | bytes accessed | tf_op | source)
XLA Modules:
  0.0 39.6 jit_solution(13005716942623207843)
XLA Ops:
  0.0 39.0 %shard_map.73 = bf16[256,128]{1,0:T(8,128)(2,1)S(1)} custom-call(bf16[256,128]{1,0:T(8,128)(2,1)} %x_hbm.1, bf16[1,128]{1,0:T(2,128)(2,1)} %gain_hbm.1, bf16[1,2048,128]{2,1,0:T(8,128)(2,1)} %wv_hbm.1, bf16[1,2048,128]{2,1,0:T(8,128)(2,1)} %wg_hbm.1, bf16[1,31,128]{2,1,0:T(8,128)(2,1)} %taps_hbm.1, f32[1,128]{1,0:T(1,128)} %lgain_hbm.1, f32[1,128]{1,0:T(1,128)} %lshift_hbm.1), custom_call_target="tpu_custom_call" | custom-call | tf_op jit(solution)/shard_map/pallas_call | solution.py:511
  39.0 0.6 %copy.9 = bf16[256,128]{1,0:T(8,128)(2,1)} copy(bf16[256,128]{1,0:T(8,128)(2,1)S(1)} %shard_map.73) | data formatting | bytes 131072

commit v5 on v4

--- a/solution.py
+++ b/solution.py
@@ -9,15 +9,15 @@
 
 LEN = 128
 SPLITS = ((128, 128), (128, 128))
-FEED = (2, 3, 1)
-SEND = (0, 3, 2, 1)
-ENTER = (0, 1, 3, 2)
+FEED = (1, 2, 3)
+SEND = (3, 0, 2, 1)
+ENTER = (0, 3, 1, 2)
 XCARRY = (1, 2, 3)
 ZRELAY = (1, 2)
 SWAP = 256
 TIMES = (
-    {"S0": (-0.48, 4.35, 10.17, 11.39), "S1": (6.67, 11.13, 17.25, 20.33), "S2": (8.5, 15.39, 18.61, 20.55), "step": (8.5, 15.39, 18.61, 20.55), "swap": (0, 0, 31.88, 26.88)},
-    {"S0": (10.67, 16.26, 7.57, 7.57), "C00": (16.08, 17.31, 18.47, 19.95), "ent": (18.0, 19.3, 21.72, 24.23), "C1": (21.04, 25.35, 26.83, 31.69), "C2": (21.81, 26.26, 31.37, 33.41), "step": (21.81, 26.27, 31.37, 33.42), "fin": (32.83, 34.11, 38.98, 44.31), "S1": (0, 0, 8.63, 11.78), "ent2": (0, 0, 29.86, 28.1)},
+    {"S0": (-0.48, 4.35, 10.17, 11.39), "S1": (6.67, 11.13, 17.25, 20.33), "S2": (8.5, 15.39, 18.61, 20.55), "step": (8.5, 15.39, 18.61, 20.55), "swap": (0, 0, 26.5, 26.88)},
+    {"S0": (10.67, 16.26, 7.57, 7.57), "C00": (16.08, 17.31, 18.47, 19.95), "ent": (18.0, 19.3, 21.72, 24.23), "C1": (21.04, 25.35, 26.83, 31.69), "C2": (21.81, 26.26, 31.37, 33.41), "step": (21.81, 26.27, 31.37, 33.42), "fin": (32.83, 33.0, 38.98, 44.31), "S1": (0, 0, 8.63, 11.78), "ent2": (0, 0, 29.86, 28.1)},
 )
 
 
@@ -187,6 +187,13 @@
     def give(n, i, start, size, cls, dev):
         send(x_ref.at[pl.ds(i, size)], sg.at[me, pl.ds(start, size)], sent.at[0], s_sem.at[n, cls], dev)
         counts[0] += size
+
+    def introduce(last):
+        if cross:
+            pl.semaphore_wait(meet_sem.at[top], 1)
+        if not last:
+            for dev in plane(k + 1):
+                send(lnp, lng.at[me], sent.at[0], gain_sem.at[1], dev)
 
     def greet():
         for dev in peers:
@@ -423,11 +430,8 @@
                 give(n, i, start, size, 0, at(1 - k, f, t))
             meet()
         greet()
-        if cross:
-            pl.semaphore_wait(meet_sem.at[top], 1)
-        if not last:
-            for dev in plane(k + 1):
-                send(lnp, lng.at[me], sent.at[0], gain_sem.at[1], dev)
+        soon = min(op[0] for op in ops)
+        ops.append((soon + 1e-6, functools.partial(introduce, last)))
         for _, op in sorted(ops, key=lambda op: op[0]):
             op()
         drain(counts[0], sent.at[0])

time: 40.2 us -> 39.9 us (level); the launches traced: 39.6 us -> 39.8 us
  no operation moved by 1% of the time
where the time goes in v5:
time: 39.9 us; the launch traced here: 39.8 us
  Pallas kernels  39.1 us (98%)
  local copies, waits for them, and re-layouts  0.63 us (2%)
    pallas_call x1, Pallas kernels, local(): pl.pallas_call(functools.partial(kernel, sizes), out_shape=pltpu.VMEM((ow...  39.1 us

profile of v5, /device:TPU:3, one launch (start us, length us, event | category | flops | bytes accessed | tf_op | source)
XLA Modules:
  0.0 39.8 jit_solution(11578054736324611337)
XLA Ops:
  0.0 39.1 %shard_map.73 = bf16[256,128]{1,0:T(8,128)(2,1)S(1)} custom-call(bf16[256,128]{1,0:T(8,128)(2,1)} %x_hbm.1, bf16[1,128]{1,0:T(2,128)(2,1)} %gain_hbm.1, bf16[1,2048,128]{2,1,0:T(8,128)(2,1)} %wv_hbm.1, bf16[1,2048,128]{2,1,0:T(8,128)(2,1)} %wg_hbm.1, bf16[1,31,128]{2,1,0:T(8,128)(2,1)} %taps_hbm.1, f32[1,128]{1,0:T(1,128)} %lgain_hbm.1, f32[1,128]{1,0:T(1,128)} %lshift_hbm.1), custom_call_target="tpu_custom_call" | custom-call | tf_op jit(solution)/shard_map/pallas_call | solution.py:515
  39.1 0.6 %copy.9 = bf16[256,128]{1,0:T(8,128)(2,1)} copy(bf16[256,128]{1,0:T(8,128)(2,1)S(1)} %shard_map.73) | data formatting | bytes 131072

commit v6 on v5

--- a/solution.py
+++ b/solution.py
@@ -481,7 +481,7 @@
 def when(chunks, own_rows, cross, kk, n, op):
     if cross and TIMES:
         if op == "prep":
-            return TIMES[kk]["C00" if kk else "step"][0] - 0.01
+            return TIMES[kk]["C00" if kk else "S1"][0] - 0.01
         return TIMES[kk][op][n]
     start, size = chunks[n]
     late = start + size

time: 39.9 us -> 39.7 us (level)
  no operation moved by 1% of the time
where the time goes in v6:
time: 39.7 us; the launch traced here: 39.6 us
  Pallas kernels  38.9 us (98%)
  local copies, waits for them, and re-layouts  0.63 us (2%)
    pallas_call x1, Pallas kernels, local(): pl.pallas_call(functools.partial(kernel, sizes), out_shape=pltpu.VMEM((ow...  38.9 us

profile of v6, /device:TPU:3, one launch (start us, length us, event | category | flops | bytes accessed | tf_op | source)
XLA Modules:
  0.0 39.6 jit_solution(4392737746001900381)
XLA Ops:
  0.0 38.9 %shard_map.73 = bf16[256,128]{1,0:T(8,128)(2,1)S(1)} custom-call(bf16[256,128]{1,0:T(8,128)(2,1)} %x_hbm.1, bf16[1,128]{1,0:T(2,128)(2,1)} %gain_hbm.1, bf16[1,2048,128]{2,1,0:T(8,128)(2,1)} %wv_hbm.1, bf16[1,2048,128]{2,1,0:T(8,128)(2,1)} %wg_hbm.1, bf16[1,31,128]{2,1,0:T(8,128)(2,1)} %taps_hbm.1, f32[1,128]{1,0:T(1,128)} %lgain_hbm.1, f32[1,128]{1,0:T(1,128)} %lshift_hbm.1), custom_call_target="tpu_custom_call" | custom-call | tf_op jit(solution)/shard_map/pallas_call | solution.py:515
  39.0 0.6 %copy.9 = bf16[256,128]{1,0:T(8,128)(2,1)} copy(bf16[256,128]{1,0:T(8,128)(2,1)S(1)} %shard_map.73) | data formatting | bytes 131072

commit v7 on v6

--- a/solution.py
+++ b/solution.py
@@ -17,7 +17,7 @@
 SWAP = 256
 TIMES = (
     {"S0": (-0.48, 4.35, 10.17, 11.39), "S1": (6.67, 11.13, 17.25, 20.33), "S2": (8.5, 15.39, 18.61, 20.55), "step": (8.5, 15.39, 18.61, 20.55), "swap": (0, 0, 26.5, 26.88)},
-    {"S0": (10.67, 16.26, 7.57, 7.57), "C00": (16.08, 17.31, 18.47, 19.95), "ent": (18.0, 19.3, 21.72, 24.23), "C1": (21.04, 25.35, 26.83, 31.69), "C2": (21.81, 26.26, 31.37, 33.41), "step": (21.81, 26.27, 31.37, 33.42), "fin": (32.83, 33.0, 38.98, 44.31), "S1": (0, 0, 8.63, 11.78), "ent2": (0, 0, 29.86, 28.1)},
+    {"S0": (10.67, 16.26, 7.57, 7.57), "C00": (16.08, 17.31, 18.47, 19.95), "ent": (18.0, 19.3, 21.72, 24.23), "C1": (21.04, 25.35, 26.83, 31.69), "C2": (21.81, 26.26, 31.37, 33.41), "step": (21.81, 26.27, 31.37, 33.42), "fin": (32.83, 34.11, 38.98, 44.31), "S1": (0, 0, 8.63, 11.78), "ent2": (0, 0, 29.86, 28.1)},
 )
 
 

time: 39.7 us -> 39.4 us (level)
  Pallas kernels: 38.9 us -> 38.4 us
    pallas_call x1, Pallas kernels: 38.9 us -> 38.4 us  [local(): pl.pallas_call(functools.partial(kernel, sizes), out_shape=pltpu.VMEM((ow...]
where the time goes in v7:
time: 39.4 us; the launch traced here: 39 us
  Pallas kernels  38.4 us (97%)
  local copies, waits for them, and re-layouts  0.63 us (2%)
    pallas_call x1, Pallas kernels, local(): pl.pallas_call(functools.partial(kernel, sizes), out_shape=pltpu.VMEM((ow...  38.4 us

profile of v7, /device:TPU:3, one launch (start us, length us, event | category | flops | bytes accessed | tf_op | source)
XLA Modules:
  0.0 39.0 jit_solution(7394473572189403420)
XLA Ops:
  0.0 38.4 %shard_map.73 = bf16[256,128]{1,0:T(8,128)(2,1)S(1)} custom-call(bf16[256,128]{1,0:T(8,128)(2,1)} %x_hbm.1, bf16[1,128]{1,0:T(2,128)(2,1)} %gain_hbm.1, bf16[1,2048,128]{2,1,0:T(8,128)(2,1)} %wv_hbm.1, bf16[1,2048,128]{2,1,0:T(8,128)(2,1)} %wg_hbm.1, bf16[1,31,128]{2,1,0:T(8,128)(2,1)} %taps_hbm.1, f32[1,128]{1,0:T(1,128)} %lgain_hbm.1, f32[1,128]{1,0:T(1,128)} %lshift_hbm.1), custom_call_target="tpu_custom_call" | custom-call | tf_op jit(solution)/shard_map/pallas_call | solution.py:515
  38.4 0.6 %copy.9 = bf16[256,128]{1,0:T(8,128)(2,1)} copy(bf16[256,128]{1,0:T(8,128)(2,1)S(1)} %shard_map.73) | data formatting | bytes 131072

commit v8 on v7

--- a/solution.py
+++ b/solution.py
@@ -127,6 +127,7 @@
     every = tuple(range(T))
     chunks, cross = plan(sizes, own_rows)
     NCH = len(chunks)
+    lead = sum(start < SWAP for start, _ in chunks)
     zrelay = ZRELAY if pow2 and T == 4 else ()
 
     def rows_of(n):
@@ -331,14 +332,14 @@
             if dt not in zrelay:
                 send(conv_out.at[rows], cg.at[me, rows], sent.at[0], c_sem.at[n, dt], at(k + 1, f, to_t[dt]))
         if swapped:
-            send(conv_out.at[rows], side.at[rows], sent.at[0], side_sem.at[n], at(k, f ^ (F // 2), t))
+            send(conv_out.at[rows], side.at[rows], sent.at[0], side_sem.at[n - lead], at(k, f ^ (F // 2), t))
         if not first:
             for dt in every:
                 send(hg.at[me, rows], sg.at[me, rows], sent.at[0], s_sem.at[n, dt], at(k + 1, f, to_t[dt]))
 
     def swap_on(n):
         rows = rows_of(n)
-        await_bytes(side.at[rows], side_sem.at[n])
+        await_bytes(side.at[rows], side_sem.at[n - lead])
         slot = (f ^ (F // 2)) * T + t
         send(side.at[rows], cg.at[slot, rows], sent.at[0], c_sem.at[n, T], at(k + 1, f, t))
 
@@ -529,7 +530,7 @@
             V((LEN, LEN), f32),
             dma((NC, T * F)) if F & (F - 1) else dma((NC, max(F // 2, 1) * T + 1)),
             dma((NC, T + 1)), dma((NC, max(F // 2 - 1, 0) * T + 1)), dma((NC,)), dma((NC,)), dma((2,)), dma((1,)),
-            dma((1,)), V((TOK, C), bf16), dma((NC,)), pltpu.SemaphoreType.REGULAR((4,)),
+            dma((1,)), V((TOK, C), bf16), dma((max(sum(c[0] >= SWAP for c in chunks), 1),)), pltpu.SemaphoreType.REGULAR((max(F.bit_length(), 1),)),
         ],
         compiler_params=pltpu.CompilerParams(collective_id=0, has_side_effects=True),
     )(*operands)

time: 39.4 us -> 39.4 us (level)
  no operation moved by 1% of the time
where the time goes in v8:
time: 39.4 us; the launch traced here: 39 us
  Pallas kernels  38.3 us (97%)
  local copies, waits for them, and re-layouts  0.63 us (2%)
    pallas_call x1, Pallas kernels, local(): pl.pallas_call(functools.partial(kernel, sizes), out_shape=pltpu.VMEM((ow...  38.3 us

profile of v8, /device:TPU:3, one launch (start us, length us, event | category | flops | bytes accessed | tf_op | source)
XLA Modules:
  0.0 39.0 jit_solution(16819681310358037466)
XLA Ops:
  0.0 38.3 %shard_map.73 = bf16[256,128]{1,0:T(8,128)(2,1)S(1)} custom-call(bf16[256,128]{1,0:T(8,128)(2,1)} %x_hbm.1, bf16[1,128]{1,0:T(2,128)(2,1)} %gain_hbm.1, bf16[1,2048,128]{2,1,0:T(8,128)(2,1)} %wv_hbm.1, bf16[1,2048,128]{2,1,0:T(8,128)(2,1)} %wg_hbm.1, bf16[1,31,128]{2,1,0:T(8,128)(2,1)} %taps_hbm.1, f32[1,128]{1,0:T(1,128)} %lgain_hbm.1, f32[1,128]{1,0:T(1,128)} %lshift_hbm.1), custom_call_target="tpu_custom_call" | custom-call | tf_op jit(solution)/shard_map/pallas_call | solution.py:516
  38.4 0.6 %copy.9 = bf16[256,128]{1,0:T(8,128)(2,1)} copy(bf16[256,128]{1,0:T(8,128)(2,1)S(1)} %shard_map.73) | data formatting | bytes 131072
